TPU v7x, 1024 devices: a whole 8x8x8 slice. The times are simulated.
1024 devices in a mesh: tp: 64 (over z, y), dp: 16 (over x, core).
Axes of the slice: x: 8, y: 8, z: 8, core: 2. Of those that a mesh axis runs over, the one named last changes fastest.
Arguments:
- stream: bfloat16 [128, 4096], P('dp', 'tp'), may hold values from -6 to 6
- query_weight: bfloat16 [2, 4096, 3072], P(None, 'dp', 'tp'), may hold values from -0.09375 to 0.09375
- key_weight: bfloat16 [2, 4096, 3072], P(None, 'dp', 'tp'), may hold values from -0.09375 to 0.09375
- value_weight: bfloat16 [2, 4096, 3072], P(None, 'dp', 'tp'), may hold values from -0.09375 to 0.09375
- outgate_weight: bfloat16 [2, 4096, 3072], P(None, 'dp', 'tp'), may hold values from -0.09375 to 0.09375
- gate_weight: bfloat16 [2, 4096, 32], replicated, may hold values from -0.09375 to 0.09375
- gate_bias: float32 [2, 32], replicated, may hold values from -1 to 3
- output_weight: bfloat16 [2, 3072, 4096], P(None, 'dp', 'tp'), may hold values from -0.109375 to 0.109375
- norm_gain: float32 [2, 4096], replicated, may hold values from 0.1 to 1.9
- matrix_state: float32 [2, 128, 192, 16, 192], P(None, 'dp', 'tp'), may hold values from -0.6 to 0.6
- normalizer_state: float32 [2, 128, 16, 192], P(None, 'dp'), may hold values from -0.6 to 0.6
- stabilizer_state: float32 [2, 128, 16], P(None, 'dp'), may hold values from -4 to 4
Outputs:
- out_stream: bfloat16 [128, 4096], P('dp', 'tp')
- new_matrix: float32 [2, 128, 192, 16, 192], P(None, 'dp', 'tp')
- new_normalizer: float32 [2, 128, 16, 192], P(None, 'dp')
- new_stabilizer: float32 [2, 128, 16], P(None, 'dp')
All inputs are finite; a program needn't handle non-finite values.
Results may differ from a plain program's by a relative error of at most 0.015.
Values may be sent and summed in bfloat16 or wider, within the bound.
No kernel may reach another device: no remote copies, remote signals or barrier semaphores. Data moves between devices by JAX's collectives and lax.ppermute only.
A program may use at most 32 MiB of HBM per device.

v0:
```python
import functools

import jax
import jax.numpy as jnp
from jax import lax
from jax.experimental import pallas as pl
from jax.experimental.pallas import tpu as pltpu
from jax.sharding import PartitionSpec as P


residual_scale = 8.0**0.25
norm_eps = 1e-05
LANES = 128
F32 = jnp.float32


def exchange(pieces, axis, groups=None):
    return lax.all_to_all(
        pieces, axis, split_axis=0, concat_axis=0, tiled=True, axis_index_groups=groups
    )


def after(x, earlier):
    return lax.optimization_barrier((x, *earlier))[0]


def step_of(held, bit):
    size = lax.axis_size("dp")
    return lax.ppermute(held, "dp", [(i, i ^ bit) for i in range(size)])


def merged(held, got):
    return lax.optimization_barrier(jnp.concatenate([held, got]))


def chain_order(size):
    held, bit = [0], size // 2
    while bit > 1:
        held = held + [h ^ bit for h in held]
        bit //= 2
    return held


def row_dot(x, turned):
    return lax.dot_general(x, turned, (((1,), (1,)), ((), ())), preferred_element_type=F32)


def blocks_dot(x_ref, halves, order, whole, low, high):
    me = lax.axis_index("dp")
    base = me if whole else me & 1
    rows = halves[0].shape[2]
    total = jnp.zeros((x_ref.shape[0], high - low), F32)
    for slot, other in enumerate(order):
        for half, ref in enumerate(halves):
            at = pl.multiple_of((base ^ (other ^ half)) * rows, rows)
            total = total + row_dot(x_ref[:, pl.ds(at, rows)], ref[slot, low:high, :])
    return total


def pair_up(pieces_ref, width, at):
    two = [pieces_ref[2 * at + k][:, :width].astype(F32) for k in range(2)]
    return jnp.concatenate(two, axis=1)


def spread(ref, x):
    if x.shape[1] < LANES:
        x = jnp.concatenate([x, jnp.zeros((x.shape[0], LANES - x.shape[1]), x.dtype)], axis=1)
    x = x.astype(ref.dtype)
    for copy in range(ref.shape[0]):
        ref[copy] = x


def call(kernel, out_shape, *arrays, flops=10**6, scratch=()):
    moved = sum(a.size * a.dtype.itemsize for a in arrays)
    return pl.pallas_call(
        kernel,
        out_shape=out_shape,
        scratch_shapes=list(scratch),
        cost_estimate=pl.CostEstimate(flops=flops, bytes_accessed=moved, transcendentals=0),
        compiler_params=pltpu.CompilerParams(vmem_limit_bytes=20 * 2**20),
    )(*arrays)


def first_kernel(order, cut, high, pieces_ref, held_ref, got_ref, x_ref, qk_ref, vo_ref):
    width = x_ref.shape[1] // pieces_ref.shape[0]
    for at in range(pieces_ref.shape[0] // 2):
        cols = slice(2 * width * at, 2 * width * (at + 1))
        x_ref[:, cols] = pair_up(pieces_ref, width, at).astype(x_ref.dtype)
    out = blocks_dot(x_ref, (held_ref, got_ref), order, False, 0, high)
    spread(qk_ref, out[:, :cut])
    vo_ref[...] = out[:, cut:].astype(vo_ref.dtype)


def norm_kernel(order, cut, high, pieces_ref, gain_ref, held_ref, got_ref, x_ref, qk_ref, vo_ref):
    count, width = pieces_ref.shape[0], x_ref.shape[1] // pieces_ref.shape[0]
    pairs = [pair_up(pieces_ref, width, at) for at in range(count // 2)]
    features = x_ref.shape[1]
    mean = jnp.sum(sum(pairs), axis=1, keepdims=True) / features
    pairs = [p - mean for p in pairs]
    variance = jnp.sum(sum(p * p for p in pairs), axis=1, keepdims=True) / features
    scale = lax.rsqrt(variance + norm_eps)
    for at, p in enumerate(pairs):
        cols = slice(2 * width * at, 2 * width * (at + 1))
        x_ref[:, cols] = (p * scale * gain_ref[:, cols]).astype(x_ref.dtype)
    out = blocks_dot(x_ref, (held_ref, got_ref), order, True, 0, high)
    spread(qk_ref, out[:, :cut])
    vo_ref[...] = out[:, cut:].astype(vo_ref.dtype)


def head_sums(x, heads):
    x = x.reshape(heads, -1, *x.shape[1:]).sum(1)
    lane = lax.broadcasted_iota(jnp.int32, (x.shape[1], LANES), 1)
    sums = jnp.sum(x, axis=2, keepdims=True)
    total = jnp.zeros((x.shape[1], LANES), F32)
    for head in range(heads):
        total = jnp.where(lane == head, sums[head], total)
    return total


def readout_kernel(scale, pieces_ref, vo_ref, retain_ref, admit_ref, state_ref, normalizer_ref, out_ref):
    heads = retain_ref.shape[1]
    width = state_ref.shape[3]
    both = pieces_ref[...].astype(F32)
    query = both[:, :, :width]
    key = both[:, :, width : 2 * width] * scale
    retain, admit = retain_ref[...], admit_ref[...]
    of_key = head_sums(query * key, heads)[:, :heads] * admit
    of_normalizer = head_sums(query * normalizer_ref[...], heads)[:, :heads] * retain
    divisor = jnp.maximum(jnp.abs(of_normalizer + of_key), 1.0)
    vo = vo_ref[...].astype(F32)
    parts = []
    for e in range(state_ref.shape[0]):
        numerator = head_sums(query * state_ref[e], heads)[:, :heads] * retain
        value = vo[:, e * heads : (e + 1) * heads]
        gate = vo[:, width + e * heads : width + (e + 1) * heads]
        parts.append((numerator + value * of_key) / divisor * jax.nn.sigmoid(gate))
    spread(out_ref, jnp.concatenate(parts, axis=1))


def branch_kernel(order, whole, low, high, pieces_ref, x_ref, held_ref, got_ref, out_ref, wide_ref):
    width = high - low
    for at in range(pieces_ref.shape[0] // 2):
        cols = slice(2 * width * at, 2 * width * (at + 1))
        wide_ref[:, cols] = pair_up(pieces_ref, width, at).astype(wide_ref.dtype)
    branch = blocks_dot(wide_ref, (held_ref, got_ref), order, whole, low, high)
    spread(out_ref, residual_scale * x_ref[...].astype(F32) + branch)


def last_kernel(features, pieces_ref, gain_ref, out_ref):
    width = out_ref.shape[1]
    pieces = [pieces_ref[at].astype(F32) for at in range(pieces_ref.shape[0])]
    mean = jnp.sum(sum(pieces), axis=1, keepdims=True) / features
    lane = lax.broadcasted_iota(jnp.int32, pieces[0].shape, 1)
    off = [jnp.where(lane < width, p - mean, 0.0) for p in pieces]
    variance = jnp.sum(sum(p * p for p in off), axis=1, keepdims=True) / features
    own = pieces_ref[lax.axis_index("tp")].astype(F32)[:, :width]
    out = (own - mean) * lax.rsqrt(variance + norm_eps) * gain_ref[...]
    out_ref[...] = out.astype(out_ref.dtype)


def update(retain, admit, values, keys, state):
    fresh = admit[:, None, :, None] * values[..., None] * keys[:, None, :, :]
    return retain[:, None, :, None] * state + fresh


def shards(
    stream,
    query_weight,
    key_weight,
    value_weight,
    outgate_weight,
    gate_weight,
    gate_bias,
    output_weight,
    norm_gain,
    matrix_state,
    normalizer_state,
    stabilizer_state,
):
    head_count = gate_bias.shape[1] // 2
    head_size = normalizer_state.shape[3]
    seqs, feats = stream.shape
    rows, cols = query_weight.shape[1:]
    peers = lax.axis_size("tp")
    owners = lax.axis_size("dp")
    order = chain_order(owners)
    by_chip = [2 * chip for chip in range(owners // 2)]
    me = lax.axis_index("tp")
    bf16 = stream.dtype
    copies = jax.ShapeDtypeStruct((peers, seqs, LANES), bf16)
    pair = jax.ShapeDtypeStruct((seqs, 2 * cols), bf16)
    per_head = head_size // cols
    turned = [jnp.swapaxes(w, 1, 2) for w in (query_weight, key_weight, value_weight, outgate_weight)]
    out_turned = jnp.swapaxes(output_weight, 1, 2).reshape(-1, feats, rows // feats, cols)
    out_turned = jnp.pad(out_turned, ((0, 0), (0, 0), (0, 0), (0, feats - cols)))
    out_turned = out_turned.reshape(-1, feats, rows)

    bulk = jnp.concatenate([w[0] for w in turned])
    chain_d = out_turned[:1]
    chain_c = jnp.concatenate([w[1] for w in turned] + [out_turned[1]])[None]

    def by_piece(x):
        x = x.reshape(*x.shape[:-1], per_head, cols)
        return jnp.moveaxis(x, 0, -2).reshape(*x.shape[1:-3], peers, seqs, cols)

    states = [by_piece(m) for m in matrix_state]
    normalizers = [by_piece(n) for n in normalizer_state]

    chips = [[2 * chip + core for chip in range(owners // 2)] for core in range(2)]
    bulk = jnp.broadcast_to(bulk, (owners // 2, *bulk.shape))
    bulk = exchange(bulk, "dp", chips)
    tile = jnp.pad(stream, ((0, 0), (0, LANES - feats)))
    tile = after(tile, (*states, *normalizers, bulk))
    pieces = exchange(jnp.broadcast_to(tile, copies.shape), "tp")
    got_bulk = step_of(bulk, 1)
    got_d = step_of(chain_d, 8)
    got_c = step_of(chain_c, 8)
    x_local = stream
    whole_x = jax.ShapeDtypeStruct((seqs, peers * feats), bf16)
    saved, new_mats, new_norms, new_stabs = ([], [], [], [])
    for block_no in range(gate_bias.shape[0]):
        if block_no == 0:
            x_full, qk, vo = call(
                functools.partial(first_kernel, by_chip, 2 * cols, 4 * cols),
                (whole_x, copies, pair),
                pieces,
                bulk,
                got_bulk,
            )
            chain_d = merged(after(chain_d, (qk,)), got_d)
            got_d = step_of(chain_d, 4)
            chain_c = merged(after(chain_c, (qk,)), got_c)
            got_c = step_of(chain_c, 4)
        else:
            x_full, qk, vo = call(
                functools.partial(norm_kernel, order, 2 * cols, 4 * cols),
                (whole_x, copies, pair),
                pieces,
                norm_gain[:1],
                chain_c,
                got_c,
            )
            x_local = lax.dynamic_slice_in_dim(x_full, me * feats, feats, 1)
            saved[0] = (*saved[0][:4], qk)
        pieces = exchange(qk, "tp")
        gate_pre = (
            jnp.dot(x_full, gate_weight[block_no], preferred_element_type=F32)
            + gate_bias[block_no]
        )
        log_in = gate_pre[:, :head_count]
        log_forget = jax.nn.log_sigmoid(gate_pre[:, head_count:])
        old_stab = stabilizer_state[block_no]
        stab_new = jnp.maximum(log_forget + old_stab, log_in)
        retain = jnp.exp(log_forget + old_stab - stab_new)
        admit = jnp.exp(log_in - stab_new)
        hidden = call(
            functools.partial(readout_kernel, head_size**-0.5),
            copies,
            pieces,
            vo,
            retain,
            admit,
            states[block_no],
            normalizers[block_no],
        )
        if block_no == 0:
            chain_d = merged(after(chain_d, (hidden,)), got_d)
            got_d = step_of(chain_d, 2)
            chain_d = merged(chain_d, got_d)
            got_d = step_of(chain_d, 1)
            chain_c = merged(after(chain_c, (hidden,)), got_c)
            got_c = step_of(chain_c, 2)
        out_halves, out_low = ((chain_d, got_d), 0) if block_no == 0 else ((chain_c, got_c), 4 * cols)
        key_pieces = pieces[:, :, cols : 2 * cols]
        saved.append((key_pieces, vo, retain, admit, hidden))
        pieces = exchange(hidden, "tp")
        summed = call(
            functools.partial(branch_kernel, order, True, out_low, out_low + feats),
            copies,
            pieces,
            x_local,
            *out_halves,
            scratch=[pltpu.VMEM((seqs, peers * feats), bf16)],
        )
        if block_no == 0:
            chain_c = merged(after(chain_c, (summed,)), got_c)
            got_c = step_of(chain_c, 1)
        new_stabs.append(stab_new)
        pieces = exchange(summed, "tp")
    gain = lax.dynamic_slice_in_dim(norm_gain[1:], me * feats, feats, 1)
    out = call(
        functools.partial(last_kernel, peers * feats),
        jax.ShapeDtypeStruct((seqs, feats), bf16),
        pieces,
        gain,
    )
    for (key_pieces, vo, retain, admit, earlier), matrix, normalizer in zip(
        saved, matrix_state, normalizer_state
    ):
        keys = after(key_pieces, (earlier,))
        keys = jnp.moveaxis(keys, 0, 1).reshape(seqs, head_count, head_size).astype(F32)
        keys = keys * head_size ** (-0.5)
        values = vo[:, :cols].astype(F32).reshape(seqs, -1, head_count)
        new_mats.append(update(retain, admit, values, keys, matrix))
        new_norms.append(retain[..., None] * normalizer + admit[..., None] * keys)
    return (out, jnp.stack(new_mats), jnp.stack(new_norms), jnp.stack(new_stabs))


def solution(mesh):
    return jax.shard_map(
        shards,
        mesh=mesh,
        in_specs=(
            P("dp", "tp"),
            P(None, "dp", "tp"),
            P(None, "dp", "tp"),
            P(None, "dp", "tp"),
            P(None, "dp", "tp"),
            P(),
            P(),
            P(None, "dp", "tp"),
            P(),
            P(None, "dp", "tp", None, None),
            P(None, "dp", None, None),
            P(None, "dp", None),
        ),
        out_specs=(
            P("dp", "tp"),
            P(None, "dp", "tp", None, None),
            P(None, "dp", None, None),
            P(None, "dp", None),
        ),
        check_vma=False,
    )
```

profile of v0, /device:TPU:16, one launch (start us, length us, event | category | flops | bytes accessed | tf_op | source)
XLA Modules:
  0.0 231.3 jit_solution(10500432183619107165)
XLA Ops:
  2.4 6.9 %all-to-all-start = ((bf16[8,192,256]{2,1,0:T(8,128)(2,1)}), bf16[8,192,256]{2,1,0:T(8,128)(2,1)S(1)}, u32[]{:S(2)}, u32[]{:S(2)}) async-start(bf16[8,192,256]{2,1,0:T(8,128)(2,1)} %broadcast_in_dim.6), calls=%async_computation | async-start | bytes 1572864 | tf_op jit(solution)/shard_map/all_to_all | solution.py:18
  9.6 7.8 %collective-permute-start.1 = (bf16[1,64,256]{2,1,0:T(8,128)(2,1)S(1)}, bf16[1,64,256]{2,1,0:T(8,128)(2,1)}, u32[]{:S(2)}, u32[]{:S(2)}) collective-permute-start(bf16[1,64,256]{2,1,0:T(8,128)(2,1)S(1)} %copy.31), channel_id=1, source_target_pairs={{0,8},{1,9},{2,10},{3,11},{4,12},{5,13},{6,14},{7,15},{8,0},{9,1},... | collective-permute-start | bytes 98312 | tf_op jit(solution)/shard_map/ppermute | solution.py:29
  22.8 8.0 %all-to-all-done.held_ref = bf16[8,192,256]{2,1,0:T(8,128)(2,1)S(1)} async-done(((bf16[8,192,256]{2,1,0:T(8,128)(2,1)}), bf16[8,192,256]{2,1,0:T(8,128)(2,1)S(1)}, u32[]{:S(2)}, u32[]{:S(2)}) %all-to-all-start) | async-done | bytes 786464 | tf_op jit(solution)/shard_map/all_to_all | solution.py:18
  30.8 1.9 collective-permute-start
  33.4 24.0 %all-to-all-start.1 = ((bf16[64,8,128]{2,1,0:T(8,128)(2,1)}), bf16[64,8,128]{2,1,0:T(8,128)(2,1)S(1)}, u32[]{:S(2)}, u32[]{:S(2)}) async-start(bf16[64,8,128]{2,1,0:T(8,128)(2,1)} %broadcast_in_dim.7), calls=%async_computation.1 | async-start | bytes 262144 | tf_op jit(solution)/shard_map/all_to_all | solution.py:18
  57.4 5.5 %collective-permute-start.5 = (bf16[1,256,256]{2,1,0:T(8,128)(2,1)S(1)}, bf16[1,256,256]{2,1,0:T(8,128)(2,1)}, u32[]{:S(2)}, u32[]{:S(2)}) collective-permute-start(bf16[1,256,256]{2,1,0:T(8,128)(2,1)S(1)} %bitcast.103), channel_id=1, source_target_pairs={{0,8},{1,9},{2,10},{3,11},{4,12},{5,13},{6,14},{7,15},{8,0},{9,1},... | collective-permute-start | bytes 393224 | tf_op jit(solution)/shard_map/ppermute | solution.py:29
  63.5 6.5 %all-to-all-done.1.pieces_ref = bf16[64,8,128]{2,1,0:T(8,128)(2,1)S(1)} async-done(((bf16[64,8,128]{2,1,0:T(8,128)(2,1)}), bf16[64,8,128]{2,1,0:T(8,128)(2,1)S(1)}, u32[]{:S(2)}, u32[]{:S(2)}) %all-to-all-start.1) | async-done | bytes 131104 | tf_op jit(solution)/shard_map/all_to_all | solution.py:18
  70.0 2.4 %shard_map.147 = (bf16[8,4096]{1,0:T(8,128)(2,1)S(1)}, bf16[64,8,128]{2,1,0:T(8,128)(2,1)}, bf16[8,96]{1,0:T(8,128)(2,1)S(1)}) custom-call(bf16[64,8,128]{2,1,0:T(8,128)(2,1)S(1)} %all-to-all-done.1.pieces_ref, bf16[8,192,256]{2,1,0:T(8,128)(2,1)S(1)} %all-to-all-done.held_ref, bf16[8,192,256]{2,1,0:T(8,128)(2,1)} %collective-permute-done.got_ref), custom_call_target="tpu_custom_call" | custom-call | flops 1000000 | bytes 1703936 | tf_op jit(solution)/shard_map/pallas_call | solution.py:75
  72.4 6.4 %all-to-all-start.2 = ((bf16[64,8,128]{2,1,0:T(8,128)(2,1)}), bf16[64,8,128]{2,1,0:T(8,128)(2,1)S(1)}, u32[]{:S(2)}, u32[]{:S(2)}) async-start(bf16[64,8,128]{2,1,0:T(8,128)(2,1)} %get-tuple-element.19), calls=%async_computation.2 | async-start | bytes 262144 | tf_op jit(solution)/shard_map/all_to_all | solution.py:18
  79.5 4.0 %collective-permute-start.2 = (bf16[2,64,256]{2,1,0:T(8,128)(2,1)S(1)}, bf16[2,64,256]{2,1,0:T(8,128)(2,1)S(1)}, u32[]{:S(2)}, u32[]{:S(2)}) collective-permute-start(bf16[2,64,256]{2,1,0:T(8,128)(2,1)S(1)} %pad_maximum_fusion.8), channel_id=1, source_target_pairs={{0,4},{1,5},{2,6},{3,7},{4,0},{5,1},{6,2},{7,3},{8,12},{9,13},{10,... | collective-permute-start | bytes 196616 | tf_op jit(solution)/shard_map/ppermute | solution.py:29
  84.5 2.7 %collective-permute-start.6 = (bf16[2,256,256]{2,1,0:T(8,128)(2,1)S(1)}, bf16[2,256,256]{2,1,0:T(8,128)(2,1)S(1)}, u32[]{:S(2)}, u32[]{:S(2)}) collective-permute-start(bf16[2,256,256]{2,1,0:T(8,128)(2,1)S(1)} %pad_maximum_fusion.4), channel_id=1, source_target_pairs={{0,4},{1,5},{2,6},{3,7},{4,0},{5,1},{6,2},{7,3},{8,12},{9,13},{10,... | collective-permute-start | bytes 786440 | tf_op jit(solution)/shard_map/ppermute | solution.py:29
  88.6 2.0 all-to-all-done.2.pieces_ref
  91.7 7.8 %collective-permute-done.6 = bf16[2,256,256]{2,1,0:T(8,128)(2,1)S(1)} collective-permute-done((bf16[2,256,256]{2,1,0:T(8,128)(2,1)S(1)}, bf16[2,256,256]{2,1,0:T(8,128)(2,1)S(1)}, u32[]{:S(2)}, u32[]{:S(2)}) %collective-permute-start.6) | collective-permute-done | bytes 262176 | tf_op jit(solution)/shard_map/ppermute | solution.py:29
  99.5 1.9 collective-permute-start.7
  101.5 3.9 %collective-permute-start.3 = (bf16[4,64,256]{2,1,0:T(8,128)(2,1)S(1)}, bf16[4,64,256]{2,1,0:T(8,128)(2,1)S(1)}, u32[]{:S(2)}, u32[]{:S(2)}) collective-permute-start(bf16[4,64,256]{2,1,0:T(8,128)(2,1)S(1)} %pad_maximum_fusion.6), channel_id=1, source_target_pairs={{0,2},{1,3},{2,0},{3,1},{4,6},{5,7},{6,4},{7,5},{8,10},{9,11},{10,... | collective-permute-start | bytes 393224 | tf_op jit(solution)/shard_map/ppermute | solution.py:29
  105.4 12.7 %collective-permute-done.3 = bf16[4,64,256]{2,1,0:T(8,128)(2,1)S(1)} collective-permute-done((bf16[4,64,256]{2,1,0:T(8,128)(2,1)S(1)}, bf16[4,64,256]{2,1,0:T(8,128)(2,1)S(1)}, u32[]{:S(2)}, u32[]{:S(2)}) %collective-permute-start.3) | collective-permute-done | bytes 131104 | tf_op jit(solution)/shard_map/ppermute | solution.py:29
  118.1 1.9 collective-permute-start.4
  120.0 12.8 %all-to-all-start.3 = ((bf16[64,8,128]{2,1,0:T(8,128)(2,1)}), bf16[64,8,128]{2,1,0:T(8,128)(2,1)S(1)}, u32[]{:S(2)}, u32[]{:S(2)}) async-start(bf16[64,8,128]{2,1,0:T(8,128)(2,1)} %shard_map.148), calls=%async_computation.3 | async-start | bytes 262144 | tf_op jit(solution)/shard_map/all_to_all | solution.py:18
  132.9 12.6 %all-to-all-done.3.pieces_ref = bf16[64,8,128]{2,1,0:T(8,128)(2,1)S(1)} async-done(((bf16[64,8,128]{2,1,0:T(8,128)(2,1)}), bf16[64,8,128]{2,1,0:T(8,128)(2,1)S(1)}, u32[]{:S(2)}, u32[]{:S(2)}) %all-to-all-start.3) | async-done | bytes 131104 | tf_op jit(solution)/shard_map/all_to_all | solution.py:18
  147.6 1.9 collective-permute-start.8
  149.6 5.2 %all-to-all-start.4 = ((bf16[64,8,128]{2,1,0:T(8,128)(2,1)}), bf16[64,8,128]{2,1,0:T(8,128)(2,1)S(1)}, u32[]{:S(2)}, u32[]{:S(2)}) async-start(bf16[64,8,128]{2,1,0:T(8,128)(2,1)} %shard_map.149), calls=%async_computation.4 | async-start | bytes 262144 | tf_op jit(solution)/shard_map/all_to_all | solution.py:18
  155.7 12.1 %all-to-all-done.4.pieces_ref = bf16[64,8,128]{2,1,0:T(8,128)(2,1)S(1)} async-done(((bf16[64,8,128]{2,1,0:T(8,128)(2,1)}), bf16[64,8,128]{2,1,0:T(8,128)(2,1)S(1)}, u32[]{:S(2)}, u32[]{:S(2)}) %all-to-all-start.4) | async-done | bytes 131104 | tf_op jit(solution)/shard_map/all_to_all | solution.py:18
  169.3 5.3 %all-to-all-start.5 = ((bf16[64,8,128]{2,1,0:T(8,128)(2,1)}), bf16[64,8,128]{2,1,0:T(8,128)(2,1)S(1)}, u32[]{:S(2)}, u32[]{:S(2)}) async-start(bf16[64,8,128]{2,1,0:T(8,128)(2,1)} %get-tuple-element.27), calls=%async_computation.5 | async-start | bytes 262144 | tf_op jit(solution)/shard_map/all_to_all | solution.py:18
  180.1 1.7 copy.29
  181.8 1.7 reshape.118
  183.5 3.0 %all-to-all-done.5.pieces_ref = bf16[64,8,128]{2,1,0:T(8,128)(2,1)S(1)} async-done(((bf16[64,8,128]{2,1,0:T(8,128)(2,1)}), bf16[64,8,128]{2,1,0:T(8,128)(2,1)S(1)}, u32[]{:S(2)}, u32[]{:S(2)}) %all-to-all-start.5) | async-done | bytes 131104 | tf_op jit(solution)/shard_map/all_to_all | solution.py:18
  187.6 9.8 %all-to-all-start.6 = ((bf16[64,8,128]{2,1,0:T(8,128)(2,1)}), bf16[64,8,128]{2,1,0:T(8,128)(2,1)S(1)}, u32[]{:S(2)}, u32[]{:S(2)}) async-start(bf16[64,8,128]{2,1,0:T(8,128)(2,1)} %shard_map.151), calls=%async_computation.6 | async-start | bytes 262144 | tf_op jit(solution)/shard_map/all_to_all | solution.py:18
  200.2 1.7 copy.30
  201.9 1.7 reshape.119
  204.7 4.6 %all-to-all-done.6.pieces_ref = bf16[64,8,128]{2,1,0:T(8,128)(2,1)S(1)} async-done(((bf16[64,8,128]{2,1,0:T(8,128)(2,1)}), bf16[64,8,128]{2,1,0:T(8,128)(2,1)S(1)}, u32[]{:S(2)}, u32[]{:S(2)}) %all-to-all-start.6) | async-done | bytes 131104 | tf_op jit(solution)/shard_map/all_to_all | solution.py:18
  210.3 8.2 %all-to-all-start.7 = ((bf16[64,8,128]{2,1,0:T(8,128)(2,1)}), bf16[64,8,128]{2,1,0:T(8,128)(2,1)S(1)}, u32[]{:S(2)}, u32[]{:S(2)}) async-start(bf16[64,8,128]{2,1,0:T(8,128)(2,1)} %shard_map.152), calls=%async_computation.7 | async-start | bytes 262144 | tf_op jit(solution)/shard_map/all_to_all | solution.py:18
  220.8 9.6 %all-to-all-done.7.pieces_ref = bf16[64,8,128]{2,1,0:T(8,128)(2,1)S(1)} async-done(((bf16[64,8,128]{2,1,0:T(8,128)(2,1)}), bf16[64,8,128]{2,1,0:T(8,128)(2,1)S(1)}, u32[]{:S(2)}, u32[]{:S(2)}) %all-to-all-start.7) | async-done | bytes 131104 | tf_op jit(solution)/shard_map/all_to_all | solution.py:18
  (121 shorter events, 31.8 us)
Async XLA Ops:
  2.4 6.9 %copy-start.12 = (bf16[2,192,64]{1,2,0:T(8,128)(2,1)S(1)}, bf16[2,192,64]{1,2,0:T(8,128)(2,1)}, u32[]{:S(2)}) copy-start(bf16[2,192,64]{1,2,0:T(8,128)(2,1)} %param.19) | copy-start | bytes 147460
  2.4 15.0 %copy-start.1 = (f32[2,8,3,16,192]{4,3,2,1,0:T(8,128)S(1)}, f32[2,8,3,16,192]{4,3,2,1,0:T(8,128)}, u32[]{:S(2)}) copy-start(f32[2,8,3,16,192]{4,3,2,1,0:T(8,128)} %param.21) | copy-start | bytes 1769476
  2.4 28.3 %all-to-all-start = ((bf16[8,192,256]{2,1,0:T(8,128)(2,1)}), bf16[8,192,256]{2,1,0:T(8,128)(2,1)S(1)}, u32[]{:S(2)}, u32[]{:S(2)}) async-start(bf16[8,192,256]{2,1,0:T(8,128)(2,1)} %broadcast_in_dim.6), calls=%async_computation | async-start | bytes 1572864 | tf_op jit(solution)/shard_map/all_to_all | solution.py:18
  9.6 69.2 %collective-permute-start.1 = (bf16[1,64,256]{2,1,0:T(8,128)(2,1)S(1)}, bf16[1,64,256]{2,1,0:T(8,128)(2,1)}, u32[]{:S(2)}, u32[]{:S(2)}) collective-permute-start(bf16[1,64,256]{2,1,0:T(8,128)(2,1)S(1)} %copy.31), channel_id=1, source_target_pairs={{0,8},{1,9},{2,10},{3,11},{4,12},{5,13},{6,14},{7,15},{8,0},{9,1},... | collective-permute-start | bytes 98312 | tf_op jit(solution)/shard_map/ppermute | solution.py:29
  19.7 1.6 copy-start.6
  22.8 9.9 %copy-start.15 = (bf16[2,256,48]{1,2,0:T(8,128)(2,1)S(1)}, bf16[2,256,48]{1,2,0:T(8,128)(2,1)}, u32[]{:S(2)}) copy-start(bf16[2,256,48]{1,2,0:T(8,128)(2,1)} %param.15) | copy-start | bytes 147460
  22.8 9.9 %copy-start.16 = (bf16[2,256,48]{1,2,0:T(8,128)(2,1)S(1)}, bf16[2,256,48]{1,2,0:T(8,128)(2,1)}, u32[]{:S(2)}) copy-start(bf16[2,256,48]{1,2,0:T(8,128)(2,1)} %param.16) | copy-start | bytes 147460
  30.8 39.2 %collective-permute-start = (bf16[8,192,256]{2,1,0:T(8,128)(2,1)S(1)}, bf16[8,192,256]{2,1,0:T(8,128)(2,1)}, u32[]{:S(2)}, u32[]{:S(2)}) collective-permute-start(bf16[8,192,256]{2,1,0:T(8,128)(2,1)S(1)} %all-to-all-done.held_ref), channel_id=1, source_target_pairs={{0,1},{1,0},{2,3},{3,2},{4,5},{5,4},{6,7},{7,6},{8,9},{9,8},{10,11... | collective-permute-start | bytes 2359304 | tf_op jit(solution)/shard_map/ppermute | solution.py:29
  33.4 36.6 %all-to-all-start.1 = ((bf16[64,8,128]{2,1,0:T(8,128)(2,1)}), bf16[64,8,128]{2,1,0:T(8,128)(2,1)S(1)}, u32[]{:S(2)}, u32[]{:S(2)}) async-start(bf16[64,8,128]{2,1,0:T(8,128)(2,1)} %broadcast_in_dim.7), calls=%async_computation.1 | async-start | bytes 262144 | tf_op jit(solution)/shard_map/all_to_all | solution.py:18
  57.4 5.6 %copy-start.23 = (f32[2,32]{1,0:T(2,128)S(1)}, f32[2,32]{1,0:T(2,128)}, u32[]{:S(2)}) copy-start(f32[2,32]{1,0:T(2,128)} %param.18) | copy-start | bytes 772
  57.4 26.1 %collective-permute-start.5 = (bf16[1,256,256]{2,1,0:T(8,128)(2,1)S(1)}, bf16[1,256,256]{2,1,0:T(8,128)(2,1)}, u32[]{:S(2)}, u32[]{:S(2)}) collective-permute-start(bf16[1,256,256]{2,1,0:T(8,128)(2,1)S(1)} %bitcast.103), channel_id=1, source_target_pairs={{0,8},{1,9},{2,10},{3,11},{4,12},{5,13},{6,14},{7,15},{8,0},{9,1},... | collective-permute-start | bytes 393224 | tf_op jit(solution)/shard_map/ppermute | solution.py:29
  72.3 14.8 %copy-start.10 = (bf16[2,4096,32]{1,2,0:T(8,128)(2,1)S(1)}, bf16[2,4096,32]{1,2,0:T(8,128)(2,1)}, u32[]{:S(2)}) copy-start(bf16[2,4096,32]{1,2,0:T(8,128)(2,1)} %param.17) | copy-start | bytes 1572868
  72.4 18.2 %all-to-all-start.2 = ((bf16[64,8,128]{2,1,0:T(8,128)(2,1)}), bf16[64,8,128]{2,1,0:T(8,128)(2,1)S(1)}, u32[]{:S(2)}, u32[]{:S(2)}) async-start(bf16[64,8,128]{2,1,0:T(8,128)(2,1)} %get-tuple-element.19), calls=%async_computation.2 | async-start | bytes 262144 | tf_op jit(solution)/shard_map/all_to_all | solution.py:18
  79.5 22.0 %collective-permute-start.2 = (bf16[2,64,256]{2,1,0:T(8,128)(2,1)S(1)}, bf16[2,64,256]{2,1,0:T(8,128)(2,1)S(1)}, u32[]{:S(2)}, u32[]{:S(2)}) collective-permute-start(bf16[2,64,256]{2,1,0:T(8,128)(2,1)S(1)} %pad_maximum_fusion.8), channel_id=1, source_target_pairs={{0,4},{1,5},{2,6},{3,7},{4,0},{5,1},{6,2},{7,3},{8,12},{9,13},{10,... | collective-permute-start | bytes 196616 | tf_op jit(solution)/shard_map/ppermute | solution.py:29
  84.5 15.0 %collective-permute-start.6 = (bf16[2,256,256]{2,1,0:T(8,128)(2,1)S(1)}, bf16[2,256,256]{2,1,0:T(8,128)(2,1)S(1)}, u32[]{:S(2)}, u32[]{:S(2)}) collective-permute-start(bf16[2,256,256]{2,1,0:T(8,128)(2,1)S(1)} %pad_maximum_fusion.4), channel_id=1, source_target_pairs={{0,4},{1,5},{2,6},{3,7},{4,0},{5,1},{6,2},{7,3},{8,12},{9,13},{10,... | collective-permute-start | bytes 786440 | tf_op jit(solution)/shard_map/ppermute | solution.py:29
  99.5 46.9 %collective-permute-start.7 = (bf16[4,256,256]{2,1,0:T(8,128)(2,1)S(1)}, bf16[4,256,256]{2,1,0:T(8,128)(2,1)}, u32[]{:S(2)}, u32[]{:S(2)}) collective-permute-start(bf16[4,256,256]{2,1,0:T(8,128)(2,1)S(1)} %pad_maximum_fusion.2), channel_id=1, source_target_pairs={{0,2},{1,3},{2,0},{3,1},{4,6},{5,7},{6,4},{7,5},{8,10},{9,11},{10,... | collective-permute-start | bytes 1572872 | tf_op jit(solution)/shard_map/ppermute | solution.py:29
  101.5 16.6 %collective-permute-start.3 = (bf16[4,64,256]{2,1,0:T(8,128)(2,1)S(1)}, bf16[4,64,256]{2,1,0:T(8,128)(2,1)S(1)}, u32[]{:S(2)}, u32[]{:S(2)}) collective-permute-start(bf16[4,64,256]{2,1,0:T(8,128)(2,1)S(1)} %pad_maximum_fusion.6), channel_id=1, source_target_pairs={{0,2},{1,3},{2,0},{3,1},{4,6},{5,7},{6,4},{7,5},{8,10},{9,11},{10,... | collective-permute-start | bytes 393224 | tf_op jit(solution)/shard_map/ppermute | solution.py:29
  118.1 27.3 %collective-permute-start.4 = (bf16[8,64,256]{2,1,0:T(8,128)(2,1)S(1)}, bf16[8,64,256]{2,1,0:T(8,128)(2,1)S(1)}, u32[]{:S(2)}, u32[]{:S(2)}) collective-permute-start(bf16[8,64,256]{2,1,0:T(8,128)(2,1)S(1)} %pad_maximum_fusion.3.held_ref), channel_id=1, source_target_pairs={{0,1},{1,0},{2,3},{3,2},{4,5},{5,4},{6,7},{7,6},{8,9},{9,8},{10,11... | collective-permute-start | bytes 786440 | tf_op jit(solution)/shard_map/ppermute | solution.py:29
  120.0 25.4 %all-to-all-start.3 = ((bf16[64,8,128]{2,1,0:T(8,128)(2,1)}), bf16[64,8,128]{2,1,0:T(8,128)(2,1)S(1)}, u32[]{:S(2)}, u32[]{:S(2)}) async-start(bf16[64,8,128]{2,1,0:T(8,128)(2,1)} %shard_map.148), calls=%async_computation.3 | async-start | bytes 262144 | tf_op jit(solution)/shard_map/all_to_all | solution.py:18
  146.4 3.1 %copy-start.17 = (f32[2,4096]{1,0:T(2,128)S(1)}, f32[2,4096]{1,0:T(2,128)}, u32[]{:S(2)}) copy-start(f32[2,4096]{1,0:T(2,128)} %param.20) | copy-start | bytes 98308
  147.6 20.2 %collective-permute-start.8 = (bf16[8,256,256]{2,1,0:T(8,128)(2,1)S(1)}, bf16[8,256,256]{2,1,0:T(8,128)(2,1)S(1)}, u32[]{:S(2)}, u32[]{:S(2)}) collective-permute-start(bf16[8,256,256]{2,1,0:T(8,128)(2,1)S(1)} %pad_maximum_fusion.held_ref), channel_id=1, source_target_pairs={{0,1},{1,0},{2,3},{3,2},{4,5},{5,4},{6,7},{7,6},{8,9},{9,8},{10,11... | collective-permute-start | bytes 3145736 | tf_op jit(solution)/shard_map/ppermute | solution.py:29
  149.6 18.2 %all-to-all-start.4 = ((bf16[64,8,128]{2,1,0:T(8,128)(2,1)}), bf16[64,8,128]{2,1,0:T(8,128)(2,1)S(1)}, u32[]{:S(2)}, u32[]{:S(2)}) async-start(bf16[64,8,128]{2,1,0:T(8,128)(2,1)} %shard_map.149), calls=%async_computation.4 | async-start | bytes 262144 | tf_op jit(solution)/shard_map/all_to_all | solution.py:18
  169.3 5.3 %copy-start.5 = (bf16[64,8,48]{2,1,0:T(8,128)(2,1)S(1)}, bf16[64,8,48]{2,1,0:T(8,128)(2,1)}, u32[]{:S(2)}) copy-start(bf16[64,8,48]{2,1,0:T(8,128)(2,1)} %slice.117) | copy-start | bytes 147460
  169.3 17.3 %all-to-all-start.5 = ((bf16[64,8,128]{2,1,0:T(8,128)(2,1)}), bf16[64,8,128]{2,1,0:T(8,128)(2,1)S(1)}, u32[]{:S(2)}, u32[]{:S(2)}) async-start(bf16[64,8,128]{2,1,0:T(8,128)(2,1)} %get-tuple-element.27), calls=%async_computation.5 | async-start | bytes 262144 | tf_op jit(solution)/shard_map/all_to_all | solution.py:18
  174.6 1.1 copy-start.11
  187.6 21.7 %all-to-all-start.6 = ((bf16[64,8,128]{2,1,0:T(8,128)(2,1)}), bf16[64,8,128]{2,1,0:T(8,128)(2,1)S(1)}, u32[]{:S(2)}, u32[]{:S(2)}) async-start(bf16[64,8,128]{2,1,0:T(8,128)(2,1)} %shard_map.151), calls=%async_computation.6 | async-start | bytes 262144 | tf_op jit(solution)/shard_map/all_to_all | solution.py:18
  199.0 4.6 %copy-start.2 = (f32[2,8,3,16,192]{4,3,2,1,0:T(8,128)S(1)}, f32[2,8,3,16,192]{4,3,2,1,0:T(8,128)}, u32[]{:S(2)}) copy-start(f32[2,8,3,16,192]{4,3,2,1,0:T(8,128)} %param.21) | copy-start | bytes 1769476
  209.3 9.2 %copy-start.8 = (f32[1,8,16,192]{3,2,1,0:T(8,128)S(1)}, f32[1,8,16,192]{3,2,1,0:T(8,128)}, u32[]{:S(2)}) copy-start(f32[1,8,16,192]{3,2,1,0:T(8,128)} %reshape.118) | copy-start | bytes 294916
  209.3 9.2 %copy-start.9 = (f32[1,8,16,192]{3,2,1,0:T(8,128)S(1)}, f32[1,8,16,192]{3,2,1,0:T(8,128)}, u32[]{:S(2)}) copy-start(f32[1,8,16,192]{3,2,1,0:T(8,128)} %reshape.119) | copy-start | bytes 294916
  209.3 9.2 %copy-start.18 = (f32[8,16]{1,0:T(8,128)S(1)}, f32[8,16]{1,0:T(8,128)}, u32[]{:S(2)}) copy-start(f32[8,16]{1,0:T(8,128)} %get-tuple-element.32) | copy-start | bytes 1540
  210.3 8.2 %copy-start.7 = (f32[2,8,16,192]{3,2,1,0:T(8,128)S(1)}, f32[2,8,16,192]{3,2,1,0:T(8,128)}, u32[]{:S(2)}) copy-start(f32[2,8,16,192]{3,2,1,0:T(8,128)} %param.22) | copy-start | bytes 589828
  210.3 20.1 %all-to-all-start.7 = ((bf16[64,8,128]{2,1,0:T(8,128)(2,1)}), bf16[64,8,128]{2,1,0:T(8,128)(2,1)S(1)}, u32[]{:S(2)}, u32[]{:S(2)}) async-start(bf16[64,8,128]{2,1,0:T(8,128)(2,1)} %shard_map.152), calls=%async_computation.7 | async-start | bytes 262144 | tf_op jit(solution)/shard_map/all_to_all | solution.py:18
  (9 other events, 7.2 us)
where the time goes:
time: 233 us; the launch traced here: 231 us
  starting transfers between devices  110 us (47%)
  waiting for transfers between devices  78.8 us (34%)
  local copies, waits for them, and re-layouts  23 us (10%)
  Pallas kernels  8.87 us (4%)
  other arithmetic  8.73 us (4%)
    all_to_all x8, starting transfers between devices, exchange(): lax.all_to_all(pieces, axis, split_axis=0, concat_axis=0, tiled=True, axi...  78.6 us
    all_to_all x8, waiting for transfers between devices, exchange(): lax.all_to_all(pieces, axis, split_axis=0, concat_axis=0, tiled=True, axi...  58.3 us
    ppermute x9, starting transfers between devices, step_of(): return lax.ppermute(held, 'dp', [(i, i ^ bit) for i in range(size)])  31.7 us
    ppermute x9, waiting for transfers between devices, step_of(): return lax.ppermute(held, 'dp', [(i, i ^ bit) for i in range(size)])  20.5 us
    pallas_call x7, Pallas kernels, call(): pl.pallas_call(kernel, out_shape=out_shape, scratch_shapes=list(scratch),...  8.87 us
    convert_element_type x4, local copies, waits for them, and re-layouts, shards(): jnp.moveaxis(keys, 0, 1).reshape(seqs, head_count, head_size).astype(F32)  6.84 us
  transfers between devices with their start and end apart: 17, of which 10 were waited for; matrix products, arithmetic and copies ran while one was open for 11% of the time, Pallas kernels for 2%

commit v1 on v0

--- a/solution.py
+++ b/solution.py
@@ -21,7 +21,7 @@
 
 
 def after(x, earlier):
-    return lax.optimization_barrier((x, *earlier))[0]
+    return lax.optimization_barrier((x, earlier))[0]
 
 
 def step_of(held, bit):
@@ -70,15 +70,25 @@
         ref[copy] = x
 
 
-def call(kernel, out_shape, *arrays, flops=10**6, scratch=()):
+def call(kernel, out_shape, *arrays, flops=10**6, scratch=(), specs=None, out_specs=None, aliases=None):
     moved = sum(a.size * a.dtype.itemsize for a in arrays)
+    extra = {} if specs is None else {"in_specs": specs, "grid": (1,)}
+    if out_specs is not None:
+        extra["out_specs"] = out_specs
     return pl.pallas_call(
         kernel,
         out_shape=out_shape,
         scratch_shapes=list(scratch),
+        input_output_aliases=aliases or {},
         cost_estimate=pl.CostEstimate(flops=flops, bytes_accessed=moved, transcendentals=0),
-        compiler_params=pltpu.CompilerParams(vmem_limit_bytes=20 * 2**20),
+        compiler_params=pltpu.CompilerParams(vmem_limit_bytes=32 * 2**20),
+        **extra,
     )(*arrays)
+
+
+def one_block(shape, at=None):
+    at = at or (0,) * len(shape)
+    return pl.BlockSpec(shape, lambda step: at)
 
 
 def first_kernel(order, cut, high, pieces_ref, held_ref, got_ref, x_ref, qk_ref, vo_ref):
@@ -158,9 +168,50 @@
     out_ref[...] = out.astype(out_ref.dtype)
 
 
-def update(retain, admit, values, keys, state):
-    fresh = admit[:, None, :, None] * values[..., None] * keys[:, None, :, :]
-    return retain[:, None, :, None] * state + fresh
+def column(row, heads):
+    at = lax.broadcasted_iota(jnp.int32, (heads, heads), 0)
+    lane = lax.broadcasted_iota(jnp.int32, (heads, heads), 1)
+    wide = jnp.broadcast_to(row, (heads, heads))
+    return jnp.sum(jnp.where(at == lane, wide, 0.0), axis=1, keepdims=True)
+
+
+def update_kernel(scale, parts, *refs):
+    pieces_ref, vo_ref, retain_ref, admit_ref, state_ref, normalizer_ref = refs[:6]
+    new_state_ref, new_normalizer_ref, rows_ref = refs[-3:]
+    _, seqs, channels, heads, size = state_ref.shape
+    width = size // parts
+    rows_ref[...] = pieces_ref[...].astype(F32).reshape(rows_ref.shape)
+    vo = vo_ref[...].astype(F32)
+    for seq in range(seqs):
+        found = [
+            rows_ref[pl.ds(seq + seqs * part, heads, stride=seqs * parts), :]
+            for part in range(parts)
+        ]
+        key = jnp.concatenate([f[:, width : 2 * width] for f in found], axis=1) * scale
+        retain = column(retain_ref[seq : seq + 1, :], heads)
+        admit = column(admit_ref[seq : seq + 1, :], heads)
+        new_normalizer_ref[0, seq] = retain * normalizer_ref[0, seq] + admit * key
+        for e in range(channels):
+            value = column(vo[seq : seq + 1, e * heads : (e + 1) * heads], heads)
+            new_state_ref[0, seq, e] = retain * state_ref[0, seq, e] + (admit * value) * key
+
+
+def update(block_no, saved, state, normalizer, made):
+    size, width = state.shape[4], saved[1].shape[1] // 2
+    blocks = [
+        one_block((1, *x.shape[1:]), (block_no,) + (0,) * (x.ndim - 1)) for x in (state, normalizer)
+    ]
+    whole = [one_block(x.shape) for x in saved]
+    arrays = (*saved, state, normalizer, *made)
+    return call(
+        functools.partial(update_kernel, size**-0.5, size // width),
+        [jax.ShapeDtypeStruct(x.shape, x.dtype) for x in (state, normalizer)],
+        *arrays,
+        scratch=[pltpu.VMEM((saved[0].shape[0] * saved[0].shape[1], LANES), F32)],
+        specs=[*whole, *blocks, *[pl.BlockSpec(memory_space=pl.ANY) for _ in made]],
+        out_specs=blocks,
+        aliases={6: 0, 7: 1} if made else None,
+    )
 
 
 def shards(
@@ -196,8 +247,7 @@
     out_turned = out_turned.reshape(-1, feats, rows)
 
     bulk = jnp.concatenate([w[0] for w in turned])
-    chain_d = out_turned[:1]
-    chain_c = jnp.concatenate([w[1] for w in turned] + [out_turned[1]])[None]
+    chain = jnp.concatenate([w[1] for w in turned] + [out_turned[0], out_turned[1]])[None]
 
     def by_piece(x):
         x = x.reshape(*x.shape[:-1], per_head, cols)
@@ -209,15 +259,16 @@
     chips = [[2 * chip + core for chip in range(owners // 2)] for core in range(2)]
     bulk = jnp.broadcast_to(bulk, (owners // 2, *bulk.shape))
     bulk = exchange(bulk, "dp", chips)
+    got = step_of(chain, 8)
     tile = jnp.pad(stream, ((0, 0), (0, LANES - feats)))
     tile = after(tile, (*states, *normalizers, bulk))
     pieces = exchange(jnp.broadcast_to(tile, copies.shape), "tp")
     got_bulk = step_of(bulk, 1)
-    got_d = step_of(chain_d, 8)
-    got_c = step_of(chain_c, 8)
+    chain = merged(after(chain, (bulk,)), got)
+    got = step_of(chain, 4)
     x_local = stream
     whole_x = jax.ShapeDtypeStruct((seqs, peers * feats), bf16)
-    saved, new_mats, new_norms, new_stabs = ([], [], [], [])
+    saved, new_stabs = ([], [])
     for block_no in range(gate_bias.shape[0]):
         if block_no == 0:
             x_full, qk, vo = call(
@@ -227,21 +278,22 @@
                 bulk,
                 got_bulk,
             )
-            chain_d = merged(after(chain_d, (qk,)), got_d)
-            got_d = step_of(chain_d, 4)
-            chain_c = merged(after(chain_c, (qk,)), got_c)
-            got_c = step_of(chain_c, 4)
+            chain = merged(after(chain, (qk,)), got)
+            got = step_of(chain, 2)
         else:
+            halves = one_block((owners // 2, 4 * cols, rows))
             x_full, qk, vo = call(
                 functools.partial(norm_kernel, order, 2 * cols, 4 * cols),
                 (whole_x, copies, pair),
                 pieces,
                 norm_gain[:1],
-                chain_c,
-                got_c,
+                chain,
+                got,
+                specs=[one_block(pieces.shape), one_block((1, peers * feats)), halves, halves],
             )
             x_local = lax.dynamic_slice_in_dim(x_full, me * feats, feats, 1)
-            saved[0] = (*saved[0][:4], qk)
+            tied = after(saved[0], (qk,))
+            made = update(0, tied, matrix_state, normalizer_state, ())
         pieces = exchange(qk, "tp")
         gate_pre = (
             jnp.dot(x_full, gate_weight[block_no], preferred_element_type=F32)
@@ -264,27 +316,21 @@
             normalizers[block_no],
         )
         if block_no == 0:
-            chain_d = merged(after(chain_d, (hidden,)), got_d)
-            got_d = step_of(chain_d, 2)
-            chain_d = merged(chain_d, got_d)
-            got_d = step_of(chain_d, 1)
-            chain_c = merged(after(chain_c, (hidden,)), got_c)
-            got_c = step_of(chain_c, 2)
-        out_halves, out_low = ((chain_d, got_d), 0) if block_no == 0 else ((chain_c, got_c), 4 * cols)
-        key_pieces = pieces[:, :, cols : 2 * cols]
-        saved.append((key_pieces, vo, retain, admit, hidden))
+            chain = merged(after(chain, (hidden,)), got)
+            got = step_of(chain, 1)
+        saved.append((pieces, vo, retain, admit))
         pieces = exchange(hidden, "tp")
+        halves = one_block((owners // 2, feats, rows), (0, 4 * cols // feats + block_no, 0))
         summed = call(
-            functools.partial(branch_kernel, order, True, out_low, out_low + feats),
+            functools.partial(branch_kernel, order, True, 0, feats),
             copies,
             pieces,
             x_local,
-            *out_halves,
+            chain,
+            got,
             scratch=[pltpu.VMEM((seqs, peers * feats), bf16)],
+            specs=[one_block(pieces.shape), one_block(x_local.shape), halves, halves],
         )
-        if block_no == 0:
-            chain_c = merged(after(chain_c, (summed,)), got_c)
-            got_c = step_of(chain_c, 1)
         new_stabs.append(stab_new)
         pieces = exchange(summed, "tp")
     gain = lax.dynamic_slice_in_dim(norm_gain[1:], me * feats, feats, 1)
@@ -294,16 +340,8 @@
         pieces,
         gain,
     )
-    for (key_pieces, vo, retain, admit, earlier), matrix, normalizer in zip(
-        saved, matrix_state, normalizer_state
-    ):
-        keys = after(key_pieces, (earlier,))
-        keys = jnp.moveaxis(keys, 0, 1).reshape(seqs, head_count, head_size).astype(F32)
-        keys = keys * head_size ** (-0.5)
-        values = vo[:, :cols].astype(F32).reshape(seqs, -1, head_count)
-        new_mats.append(update(retain, admit, values, keys, matrix))
-        new_norms.append(retain[..., None] * normalizer + admit[..., None] * keys)
-    return (out, jnp.stack(new_mats), jnp.stack(new_norms), jnp.stack(new_stabs))
+    made = update(1, after(saved[1], (summed,)), matrix_state, normalizer_state, made)
+    return (out, *made, jnp.stack(new_stabs))
 
 
 def solution(mesh):

time: 233 us -> 222 us (0.953)
  the two profiles are of different devices: /device:TPU:16 before, /device:TPU:14 now
where the time goes in v1:
time: 222 us; the launch traced here: 221 us
  waiting for transfers between devices  58.8 us (26%)
  starting transfers between devices  58.6 us (26%)
  blocking collectives  52.6 us (24%)
  local copies, waits for them, and re-layouts  29 us (13%)
  Pallas kernels  12.5 us (6%)
  other arithmetic  5.8 us (3%)
  matrix products  2.25 us (1%)
    all_to_all x6, waiting for transfers between devices, exchange(): lax.all_to_all(pieces, axis, split_axis=0, concat_axis=0, tiled=True, axi...  58.4 us
    all_to_all x2, blocking collectives, exchange(): lax.all_to_all(pieces, axis, split_axis=0, concat_axis=0, tiled=True, axi...  52.6 us
    all_to_all x6, starting transfers between devices, exchange(): lax.all_to_all(pieces, axis, split_axis=0, concat_axis=0, tiled=True, axi...  42.3 us
    ppermute x5, starting transfers between devices, step_of(): return lax.ppermute(held, 'dp', [(i, i ^ bit) for i in range(size)])  16.3 us
    pallas_call x9, Pallas kernels, call(): pl.pallas_call(kernel, out_shape=out_shape, scratch_shapes=list(scratch),...  12.5 us
    another operation x8, local copies, waits for them, and re-layouts, by_piece(): x = x.reshape(*x.shape[:-1], per_head, cols)  12.4 us
    unnamed x66, local copies, waits for them, and re-layouts  9.07 us
  transfers between devices with their start and end apart: 11, of which 7 were waited for; matrix products, arithmetic and copies ran while one was open for 11% of the time, Pallas kernels for 3%

profile of v1, /device:TPU:14, one launch (start us, length us, event | category | flops | bytes accessed | tf_op | source)
XLA Modules:
  0.0 220.5 jit_solution(387093177272217289)
XLA Ops:
  3.1 16.6 %all-to-all-start = ((bf16[8,192,256]{2,1,0:T(8,128)(2,1)}), bf16[8,192,256]{2,1,0:T(8,128)(2,1)S(1)}, u32[]{:S(2)}, u32[]{:S(2)}) async-start(bf16[8,192,256]{2,1,0:T(8,128)(2,1)} %broadcast_in_dim.9), calls=%async_computation | async-start | bytes 1572864 | tf_op jit(solution)/shard_map/all_to_all | solution.py:18
  20.2 5.1 %collective-permute-start.1 = (bf16[1,320,256]{2,1,0:T(8,128)(2,1)S(1)}, bf16[1,320,256]{2,1,0:T(8,128)(2,1)S(1)}, u32[]{:S(2)}, u32[]{:S(2)}) collective-permute-start(bf16[1,320,256]{2,1,0:T(8,128)(2,1)S(1)} %bitcast.93), channel_id=1, source_target_pairs={{0,8},{1,9},{2,10},{3,11},{4,12},{5,13},{6,14},{7,15},{8,0},{9,1},... | collective-permute-start | bytes 491528 | tf_op jit(solution)/shard_map/ppermute | solution.py:29
  25.4 10.7 %all-to-all-done.held_ref = bf16[8,192,256]{2,1,0:T(8,128)(2,1)S(1)} async-done(((bf16[8,192,256]{2,1,0:T(8,128)(2,1)}), bf16[8,192,256]{2,1,0:T(8,128)(2,1)S(1)}, u32[]{:S(2)}, u32[]{:S(2)}) %all-to-all-start) | async-done | bytes 786464 | tf_op jit(solution)/shard_map/all_to_all | solution.py:18
  36.0 1.9 collective-permute-start
  39.9 1.9 collective-permute-start.2
  41.9 1.3 reshape_unstack.12
  43.1 1.6 copy.22
  44.7 2.3 %reshape_unstack.13 = f32[8,3,16,4,48]{4,3,2,1,0:T(4,128)} reshape(f32[1,8,3,16,192]{4,3,2,1,0:T(8,128)} %get-tuple-element.48) | data formatting | bytes 589824 | tf_op jit(solution)/shard_map/reshape;unstack | solution.py:253
  47.0 2.5 %copy.23 = f32[8,3,16,4,48]{4,0,3,2,1:T(8,128)} copy(f32[8,3,16,4,48]{4,3,2,1,0:T(4,128)} %reshape_unstack.13) | data formatting | bytes 589824 | tf_op jit(solution)/shard_map/reshape;unstack | solution.py:253
  52.4 1.8 copy.25
  54.3 35.3 %all_to_all.40.pieces_ref = bf16[64,8,128]{2,1,0:T(8,128)(2,1)S(1)} all-to-all(bf16[64,8,128]{2,1,0:T(8,128)(2,1)S(1)} %broadcast_in_dim.10), channel_id=1, replica_groups=mesh['tp'=64,'dp'=16] {'tp'}, dimensions={0} | all-to-all | bytes 262144 | tf_op jit(solution)/shard_map/all_to_all | solution.py:18
  91.9 5.4 %collective-permute-start.3 = (bf16[4,320,256]{2,1,0:T(8,128)(2,1)S(1)}, bf16[4,320,256]{2,1,0:T(8,128)(2,1)}, u32[]{:S(2)}, u32[]{:S(2)}) collective-permute-start(bf16[4,320,256]{2,1,0:T(8,128)(2,1)S(1)} %pad_maximum_fusion.1), channel_id=1, source_target_pairs={{0,2},{1,3},{2,0},{3,1},{4,6},{5,7},{6,4},{7,5},{8,10},{9,11},{10,... | collective-permute-start | bytes 1966088 | tf_op jit(solution)/shard_map/ppermute | solution.py:29
  97.9 4.6 %all-to-all-start.2 = ((bf16[64,8,128]{2,1,0:T(8,128)(2,1)}), bf16[64,8,128]{2,1,0:T(8,128)(2,1)S(1)}, u32[]{:S(2)}, u32[]{:S(2)}) async-start(bf16[64,8,128]{2,1,0:T(8,128)(2,1)} %get-tuple-element.27), calls=%async_computation.2 | async-start | bytes 262144 | tf_op jit(solution)/shard_map/all_to_all | solution.py:18
  104.3 10.9 %all-to-all-done.2.pieces_ref.refs_0_ = bf16[64,8,128]{2,1,0:T(8,128)(2,1)S(1)} async-done(((bf16[64,8,128]{2,1,0:T(8,128)(2,1)}), bf16[64,8,128]{2,1,0:T(8,128)(2,1)S(1)}, u32[]{:S(2)}, u32[]{:S(2)}) %all-to-all-start.2) | async-done | bytes 131104 | tf_op jit(solution)/shard_map/all_to_all | solution.py:18
  117.0 1.9 collective-permute-start.4
  118.9 17.3 %all_to_all.41.pieces_ref = bf16[64,8,128]{2,1,0:T(8,128)(2,1)S(1)} all-to-all(bf16[64,8,128]{2,1,0:T(8,128)(2,1)S(1)} %shard_map.148), channel_id=1, replica_groups=mesh['tp'=64,'dp'=16] {'tp'}, dimensions={0} | all-to-all | bytes 262144 | tf_op jit(solution)/shard_map/all_to_all | solution.py:18
  137.2 5.5 %all-to-all-start.4 = ((bf16[64,8,128]{2,1,0:T(8,128)(2,1)}), bf16[64,8,128]{2,1,0:T(8,128)(2,1)}, u32[]{:S(2)}, u32[]{:S(2)}) async-start(bf16[64,8,128]{2,1,0:T(8,128)(2,1)} %copy-done.7), calls=%async_computation.4 | async-start | bytes 262144 | tf_op jit(solution)/shard_map/all_to_all | solution.py:18
  142.6 1.5 fusion.16
  144.1 11.1 %all-to-all-done.4.pieces_ref = bf16[64,8,128]{2,1,0:T(8,128)(2,1)} async-done(((bf16[64,8,128]{2,1,0:T(8,128)(2,1)}), bf16[64,8,128]{2,1,0:T(8,128)(2,1)}, u32[]{:S(2)}, u32[]{:S(2)}) %all-to-all-start.4) | async-done | bytes 131104 | tf_op jit(solution)/shard_map/all_to_all | solution.py:18
  155.2 1.8 shard_map.150
  158.8 5.5 %all-to-all-start.5 = ((bf16[64,8,128]{2,1,0:T(8,128)(2,1)}), bf16[64,8,128]{2,1,0:T(8,128)(2,1)}, u32[]{:S(2)}, u32[]{:S(2)}) async-start(bf16[64,8,128]{2,1,0:T(8,128)(2,1)} %copy-done.8), calls=%async_computation.5 | async-start | bytes 262144 | tf_op jit(solution)/shard_map/all_to_all | solution.py:18
  165.4 1.4 fusion.13
  166.8 10.1 %all-to-all-done.5.pieces_ref.refs_0_ = bf16[64,8,128]{2,1,0:T(8,128)(2,1)} async-done(((bf16[64,8,128]{2,1,0:T(8,128)(2,1)}), bf16[64,8,128]{2,1,0:T(8,128)(2,1)}, u32[]{:S(2)}, u32[]{:S(2)}) %all-to-all-start.5) | async-done | bytes 131104 | tf_op jit(solution)/shard_map/all_to_all | solution.py:18
  179.6 1.3 shard_map.151
  181.6 5.5 %all-to-all-start.6 = ((bf16[64,8,128]{2,1,0:T(8,128)(2,1)}), bf16[64,8,128]{2,1,0:T(8,128)(2,1)}, u32[]{:S(2)}, u32[]{:S(2)}) async-start(bf16[64,8,128]{2,1,0:T(8,128)(2,1)} %copy-done.6), calls=%async_computation.6 | async-start | bytes 262144 | tf_op jit(solution)/shard_map/all_to_all | solution.py:18
  187.1 1.3 constant_dynamic-slice_fusion.1.x_ref
  188.5 11.2 %all-to-all-done.6.pieces_ref = bf16[64,8,128]{2,1,0:T(8,128)(2,1)} async-done(((bf16[64,8,128]{2,1,0:T(8,128)(2,1)}), bf16[64,8,128]{2,1,0:T(8,128)(2,1)}, u32[]{:S(2)}, u32[]{:S(2)}) %all-to-all-start.6) | async-done | bytes 131104 | tf_op jit(solution)/shard_map/all_to_all | solution.py:18
  200.3 1.2 shard_map.152
  202.2 4.7 %all-to-all-start.7 = ((bf16[64,8,128]{2,1,0:T(8,128)(2,1)}), bf16[64,8,128]{2,1,0:T(8,128)(2,1)S(1)}, u32[]{:S(2)}, u32[]{:S(2)}) async-start(bf16[64,8,128]{2,1,0:T(8,128)(2,1)} %copy-done.5), calls=%async_computation.7 | async-start | bytes 262144 | tf_op jit(solution)/shard_map/all_to_all | solution.py:18
  209.3 2.2 shard_map.154
  212.1 3.1 %shard_map.155 = (f32[2,8,3,16,192]{4,3,2,1,0:T(8,128)}, f32[2,8,16,192]{3,2,1,0:T(8,128)}) custom-call(bf16[64,8,128]{2,1,0:T(8,128)(2,1)} %all-to-all-done.5.pieces_ref.refs_0_, bf16[8,96]{1,0:T(8,128)(2,1)S(1)} %copy-done.18, f32[8,16]{1,0:T(8,128)S(1)} %get-tuple-element.38.retain_ref.refs_2_, ...), custom_call_target="tpu_custom_call", output_to_operand_aliasing={{0}: (6, {}), {1}: (7, {})} | custom-call | flops 1000000 | bytes 1706496 | tf_op jit(solution)/shard_map/pallas_call | solution.py:78
  215.2 4.4 %all-to-all-done.7.pieces_ref = bf16[64,8,128]{2,1,0:T(8,128)(2,1)S(1)} async-done(((bf16[64,8,128]{2,1,0:T(8,128)(2,1)}), bf16[64,8,128]{2,1,0:T(8,128)(2,1)S(1)}, u32[]{:S(2)}, u32[]{:S(2)}) %all-to-all-start.7) | async-done | bytes 131104 | tf_op jit(solution)/shard_map/all_to_all | solution.py:18
  (99 shorter events, 26.6 us)
Async XLA Ops:
  2.2 17.6 %copy-start.21 = (bf16[2,192,64]{1,2,0:T(8,128)(2,1)S(1)}, bf16[2,192,64]{1,2,0:T(8,128)(2,1)}, u32[]{:S(2)}) copy-start(bf16[2,192,64]{1,2,0:T(8,128)(2,1)} %param.19) | copy-start | bytes 147460
  2.2 17.9 %copy-start.22 = (bf16[2,256,48]{1,2,0:T(8,128)(2,1)S(1)}, bf16[2,256,48]{1,2,0:T(8,128)(2,1)}, u32[]{:S(2)}) copy-start(bf16[2,256,48]{1,2,0:T(8,128)(2,1)} %param.13) | copy-start | bytes 147460
  3.1 17.0 %copy-start.23 = (bf16[2,256,48]{1,2,0:T(8,128)(2,1)S(1)}, bf16[2,256,48]{1,2,0:T(8,128)(2,1)}, u32[]{:S(2)}) copy-start(bf16[2,256,48]{1,2,0:T(8,128)(2,1)} %param.14) | copy-start | bytes 147460
  3.1 17.0 %copy-start.24 = (bf16[2,256,48]{1,2,0:T(8,128)(2,1)S(1)}, bf16[2,256,48]{1,2,0:T(8,128)(2,1)}, u32[]{:S(2)}) copy-start(bf16[2,256,48]{1,2,0:T(8,128)(2,1)} %param.15) | copy-start | bytes 147460
  3.1 17.1 %copy-start.25 = (bf16[2,256,48]{1,2,0:T(8,128)(2,1)S(1)}, bf16[2,256,48]{1,2,0:T(8,128)(2,1)}, u32[]{:S(2)}) copy-start(bf16[2,256,48]{1,2,0:T(8,128)(2,1)} %param.16) | copy-start | bytes 147460
  3.1 34.8 %copy-start = (f32[2,8,3,16,192]{4,3,2,1,0:T(8,128)S(1)}, f32[2,8,3,16,192]{4,3,2,1,0:T(8,128)}, u32[]{:S(2)}) copy-start(f32[2,8,3,16,192]{4,3,2,1,0:T(8,128)} %refs_4_.3) | copy-start | bytes 1769476
  3.1 32.9 %all-to-all-start = ((bf16[8,192,256]{2,1,0:T(8,128)(2,1)}), bf16[8,192,256]{2,1,0:T(8,128)(2,1)S(1)}, u32[]{:S(2)}, u32[]{:S(2)}) async-start(bf16[8,192,256]{2,1,0:T(8,128)(2,1)} %broadcast_in_dim.9), calls=%async_computation | async-start | bytes 1572864 | tf_op jit(solution)/shard_map/all_to_all | solution.py:18
  20.0 21.8 %copy-start.2 = (f32[2,8,16,192]{3,2,1,0:T(8,128)S(1)}, f32[2,8,16,192]{3,2,1,0:T(8,128)}, u32[]{:S(2)}) copy-start(f32[2,8,16,192]{3,2,1,0:T(8,128)} %refs_5_.3) | copy-start | bytes 589828
  20.2 18.9 %collective-permute-start.1 = (bf16[1,320,256]{2,1,0:T(8,128)(2,1)S(1)}, bf16[1,320,256]{2,1,0:T(8,128)(2,1)S(1)}, u32[]{:S(2)}, u32[]{:S(2)}) collective-permute-start(bf16[1,320,256]{2,1,0:T(8,128)(2,1)S(1)} %bitcast.93), channel_id=1, source_target_pairs={{0,8},{1,9},{2,10},{3,11},{4,12},{5,13},{6,14},{7,15},{8,0},{9,1},... | collective-permute-start | bytes 491528 | tf_op jit(solution)/shard_map/ppermute | solution.py:29
  36.0 53.5 %collective-permute-start = (bf16[8,192,256]{2,1,0:T(8,128)(2,1)S(1)}, bf16[8,192,256]{2,1,0:T(8,128)(2,1)S(1)}, u32[]{:S(2)}, u32[]{:S(2)}) collective-permute-start(bf16[8,192,256]{2,1,0:T(8,128)(2,1)S(1)} %all-to-all-done.held_ref), channel_id=1, source_target_pairs={{0,1},{1,0},{2,3},{3,2},{4,5},{5,4},{6,7},{7,6},{8,9},{9,8},{10,11... | collective-permute-start | bytes 2359304 | tf_op jit(solution)/shard_map/ppermute | solution.py:29
  39.9 50.9 %collective-permute-start.2 = (bf16[2,320,256]{2,1,0:T(8,128)(2,1)}, bf16[2,320,256]{2,1,0:T(8,128)(2,1)}, u32[]{:S(2)}, u32[]{:S(2)}) collective-permute-start(bf16[2,320,256]{2,1,0:T(8,128)(2,1)} %pad_maximum_fusion.2), channel_id=1, source_target_pairs={{0,4},{1,5},{2,6},{3,7},{4,0},{5,1},{6,2},{7,3},{8,12},{9,13},{10,... | collective-permute-start | bytes 983048 | tf_op jit(solution)/shard_map/ppermute | solution.py:29
  49.5 4.7 %copy-start.19 = (bf16[8,64]{1,0:T(8,128)(2,1)S(1)}, bf16[8,64]{1,0:T(8,128)(2,1)}, u32[]{:S(2)}) copy-start(bf16[8,64]{1,0:T(8,128)(2,1)} %x_ref.1) | copy-start | bytes 3076
  89.5 7.8 %copy-start.29 = (f32[2,32]{1,0:T(2,128)S(1)}, f32[2,32]{1,0:T(2,128)}, u32[]{:S(2)}) copy-start(f32[2,32]{1,0:T(2,128)} %param.18) | copy-start | bytes 772
  90.8 24.9 %copy-start.14 = (bf16[8,96]{1,0:T(8,128)(2,1)}, bf16[8,96]{1,0:T(8,128)(2,1)S(1)}, u32[]{:S(2)}) copy-start(bf16[8,96]{1,0:T(8,128)(2,1)S(1)} %get-tuple-element.41.vo_ref.refs_1_) | copy-start | bytes 4612
  90.8 12.9 %copy-start.28 = (f32[2,8,16]{2,1,0:T(8,128)S(1)}, f32[2,8,16]{2,1,0:T(8,128)}, u32[]{:S(2)}) copy-start(f32[2,8,16]{2,1,0:T(8,128)} %param.23) | copy-start | bytes 3076
  91.9 23.8 %collective-permute-start.3 = (bf16[4,320,256]{2,1,0:T(8,128)(2,1)S(1)}, bf16[4,320,256]{2,1,0:T(8,128)(2,1)}, u32[]{:S(2)}, u32[]{:S(2)}) collective-permute-start(bf16[4,320,256]{2,1,0:T(8,128)(2,1)S(1)} %pad_maximum_fusion.1), channel_id=1, source_target_pairs={{0,2},{1,3},{2,0},{3,1},{4,6},{5,7},{6,4},{7,5},{8,10},{9,11},{10,... | collective-permute-start | bytes 1966088 | tf_op jit(solution)/shard_map/ppermute | solution.py:29
  97.9 17.4 %all-to-all-start.2 = ((bf16[64,8,128]{2,1,0:T(8,128)(2,1)}), bf16[64,8,128]{2,1,0:T(8,128)(2,1)S(1)}, u32[]{:S(2)}, u32[]{:S(2)}) async-start(bf16[64,8,128]{2,1,0:T(8,128)(2,1)} %get-tuple-element.27), calls=%async_computation.2 | async-start | bytes 262144 | tf_op jit(solution)/shard_map/all_to_all | solution.py:18
  104.3 11.4 %copy-start.10 = (f32[8,16]{1,0:T(8,128)}, f32[8,16]{1,0:T(8,128)S(1)}, u32[]{:S(2)}) copy-start(f32[8,16]{1,0:T(8,128)S(1)} %get-tuple-element.43.admit_ref.refs_3_) | copy-start | bytes 1540
  104.3 11.4 %copy-start.12 = (f32[8,16]{1,0:T(8,128)}, f32[8,16]{1,0:T(8,128)S(1)}, u32[]{:S(2)}) copy-start(f32[8,16]{1,0:T(8,128)S(1)} %get-tuple-element.42.retain_ref.refs_2_) | copy-start | bytes 1540
  117.0 19.2 %collective-permute-start.4 = (bf16[8,320,256]{2,1,0:T(8,128)(2,1)S(1)}, bf16[8,320,256]{2,1,0:T(8,128)(2,1)S(1)}, u32[]{:S(2)}, u32[]{:S(2)}) collective-permute-start(bf16[8,320,256]{2,1,0:T(8,128)(2,1)S(1)} %pad_maximum_fusion.held_ref), channel_id=1, source_target_pairs={{0,1},{1,0},{2,3},{3,2},{4,5},{5,4},{6,7},{7,6},{8,9},{9,8},{10,11... | collective-permute-start | bytes 3932168 | tf_op jit(solution)/shard_map/ppermute | solution.py:29
  137.2 18.1 %all-to-all-start.4 = ((bf16[64,8,128]{2,1,0:T(8,128)(2,1)}), bf16[64,8,128]{2,1,0:T(8,128)(2,1)}, u32[]{:S(2)}, u32[]{:S(2)}) async-start(bf16[64,8,128]{2,1,0:T(8,128)(2,1)} %copy-done.7), calls=%async_computation.4 | async-start | bytes 262144 | tf_op jit(solution)/shard_map/all_to_all | solution.py:18
  158.8 18.0 %all-to-all-start.5 = ((bf16[64,8,128]{2,1,0:T(8,128)(2,1)}), bf16[64,8,128]{2,1,0:T(8,128)(2,1)}, u32[]{:S(2)}, u32[]{:S(2)}) async-start(bf16[64,8,128]{2,1,0:T(8,128)(2,1)} %copy-done.8), calls=%async_computation.5 | async-start | bytes 262144 | tf_op jit(solution)/shard_map/all_to_all | solution.py:18
  176.9 1.1 copy-start.1
  178.0 0.9 copy-start.4
  181.6 18.0 %all-to-all-start.6 = ((bf16[64,8,128]{2,1,0:T(8,128)(2,1)}), bf16[64,8,128]{2,1,0:T(8,128)(2,1)}, u32[]{:S(2)}, u32[]{:S(2)}) async-start(bf16[64,8,128]{2,1,0:T(8,128)(2,1)} %copy-done.6), calls=%async_computation.6 | async-start | bytes 262144 | tf_op jit(solution)/shard_map/all_to_all | solution.py:18
  188.5 19.2 %copy-start.11 = (f32[8,16]{1,0:T(8,128)S(1)}, f32[8,16]{1,0:T(8,128)}, u32[]{:S(2)}) copy-start(f32[8,16]{1,0:T(8,128)} %copy-done.10) | copy-start | bytes 1540
  188.5 19.2 %copy-start.13 = (f32[8,16]{1,0:T(8,128)S(1)}, f32[8,16]{1,0:T(8,128)}, u32[]{:S(2)}) copy-start(f32[8,16]{1,0:T(8,128)} %copy-done.12) | copy-start | bytes 1540
  202.2 9.3 %copy-start.26 = (f32[1,8,16]{2,1,0:T(8,128)S(1)}, f32[1,8,16]{2,1,0:T(8,128)}, u32[]{:S(2)}) copy-start(f32[1,8,16]{2,1,0:T(8,128)} %get-tuple-element.56) | copy-start | bytes 1540
  202.2 9.3 %copy-start.27 = (f32[1,8,16]{2,1,0:T(8,128)S(1)}, f32[1,8,16]{2,1,0:T(8,128)}, u32[]{:S(2)}) copy-start(f32[1,8,16]{2,1,0:T(8,128)} %get-tuple-element.59) | copy-start | bytes 1540
  202.2 9.9 %copy-start.18 = (bf16[8,96]{1,0:T(8,128)(2,1)S(1)}, bf16[8,96]{1,0:T(8,128)(2,1)}, u32[]{:S(2)}) copy-start(bf16[8,96]{1,0:T(8,128)(2,1)} %copy-done.16) | copy-start | bytes 4612
  202.2 17.4 %all-to-all-start.7 = ((bf16[64,8,128]{2,1,0:T(8,128)(2,1)}), bf16[64,8,128]{2,1,0:T(8,128)(2,1)S(1)}, u32[]{:S(2)}, u32[]{:S(2)}) async-start(bf16[64,8,128]{2,1,0:T(8,128)(2,1)} %copy-done.5), calls=%async_computation.7 | async-start | bytes 262144 | tf_op jit(solution)/shard_map/all_to_all | solution.py:18
  207.7 1.0 copy-start.3
  (9 other events, 5.9 us)

commit v2 on v1

--- a/solution.py
+++ b/solution.py
@@ -45,16 +45,36 @@
     return lax.dot_general(x, turned, (((1,), (1,)), ((), ())), preferred_element_type=F32)
 
 
-def blocks_dot(x_ref, halves, order, whole, low, high):
-    me = lax.axis_index("dp")
-    base = me if whole else me & 1
-    rows = halves[0].shape[2]
-    total = jnp.zeros((x_ref.shape[0], high - low), F32)
-    for slot, other in enumerate(order):
-        for half, ref in enumerate(halves):
-            at = pl.multiple_of((base ^ (other ^ half)) * rows, rows)
-            total = total + row_dot(x_ref[:, pl.ds(at, rows)], ref[slot, low:high, :])
-    return total
+class Weights:
+    def __init__(self, low, high, order, whole, held_ref, got_ref, buffer_ref, sems):
+        self.order, self.whole, self.buffer = order, whole, buffer_ref
+        self.copies = [
+            pltpu.make_async_copy(ref.at[:, low:high, :], buffer_ref.at[half], sems.at[half])
+            for half, ref in enumerate((held_ref, got_ref))
+        ]
+        for copy in self.copies:
+            copy.start()
+
+    def dot(self, x_ref):
+        me = lax.axis_index("dp")
+        base = me if self.whole else me & 1
+        rows = self.buffer.shape[3]
+        total = jnp.zeros((x_ref.shape[-2], self.buffer.shape[2]), F32)
+        for half, copy in enumerate(self.copies):
+            copy.wait()
+            for slot, other in enumerate(self.order):
+                at = base ^ (other ^ half)
+                if len(x_ref.shape) == 3:
+                    total = total + row_dot(x_ref[at], self.buffer[half, slot])
+                else:
+                    at = pl.multiple_of(at * rows, rows)
+                    total = total + row_dot(x_ref[:, pl.ds(at, rows)], self.buffer[half, slot])
+        return total
+
+
+def weight_space(held, columns):
+    shape = (2, held.shape[0], columns, held.shape[2])
+    return [pltpu.VMEM(shape, held.dtype), pltpu.SemaphoreType.DMA((2,))]
 
 
 def pair_up(pieces_ref, width, at):
@@ -72,7 +92,9 @@
 
 def call(kernel, out_shape, *arrays, flops=10**6, scratch=(), specs=None, out_specs=None, aliases=None):
     moved = sum(a.size * a.dtype.itemsize for a in arrays)
-    extra = {} if specs is None else {"in_specs": specs, "grid": (1,)}
+    extra = {} if specs is None else {"in_specs": specs}
+    if out_specs is not None:
+        extra["grid"] = (1,)
     if out_specs is not None:
         extra["out_specs"] = out_specs
     return pl.pallas_call(
@@ -91,17 +113,19 @@
     return pl.BlockSpec(shape, lambda step: at)
 
 
-def first_kernel(order, cut, high, pieces_ref, held_ref, got_ref, x_ref, qk_ref, vo_ref):
+def first_kernel(cut, fetch, pieces_ref, held_ref, got_ref, x_ref, qk_ref, vo_ref, *space):
+    weights = Weights(*fetch, held_ref, got_ref, *space)
     width = x_ref.shape[1] // pieces_ref.shape[0]
     for at in range(pieces_ref.shape[0] // 2):
         cols = slice(2 * width * at, 2 * width * (at + 1))
         x_ref[:, cols] = pair_up(pieces_ref, width, at).astype(x_ref.dtype)
-    out = blocks_dot(x_ref, (held_ref, got_ref), order, False, 0, high)
+    out = weights.dot(x_ref)
     spread(qk_ref, out[:, :cut])
     vo_ref[...] = out[:, cut:].astype(vo_ref.dtype)
 
 
-def norm_kernel(order, cut, high, pieces_ref, gain_ref, held_ref, got_ref, x_ref, qk_ref, vo_ref):
+def norm_kernel(cut, fetch, pieces_ref, gain_ref, held_ref, got_ref, x_ref, qk_ref, vo_ref, *space):
+    weights = Weights(*fetch, held_ref, got_ref, *space)
     count, width = pieces_ref.shape[0], x_ref.shape[1] // pieces_ref.shape[0]
     pairs = [pair_up(pieces_ref, width, at) for at in range(count // 2)]
     features = x_ref.shape[1]
@@ -112,7 +136,7 @@
     for at, p in enumerate(pairs):
         cols = slice(2 * width * at, 2 * width * (at + 1))
         x_ref[:, cols] = (p * scale * gain_ref[:, cols]).astype(x_ref.dtype)
-    out = blocks_dot(x_ref, (held_ref, got_ref), order, True, 0, high)
+    out = weights.dot(x_ref)
     spread(qk_ref, out[:, :cut])
     vo_ref[...] = out[:, cut:].astype(vo_ref.dtype)
 
@@ -127,12 +151,16 @@
     return total
 
 
+def side_pairs(x):
+    return jnp.stack([jnp.concatenate([x[at], x[at + 1]], axis=1) for at in range(0, len(x), 2)])
+
+
 def readout_kernel(scale, pieces_ref, vo_ref, retain_ref, admit_ref, state_ref, normalizer_ref, out_ref):
     heads = retain_ref.shape[1]
-    width = state_ref.shape[3]
+    width = vo_ref.shape[1] // 2
     both = pieces_ref[...].astype(F32)
-    query = both[:, :, :width]
-    key = both[:, :, width : 2 * width] * scale
+    query = side_pairs(both[:, :, :width])
+    key = side_pairs(both[:, :, width : 2 * width]) * scale
     retain, admit = retain_ref[...], admit_ref[...]
     of_key = head_sums(query * key, heads)[:, :heads] * admit
     of_normalizer = head_sums(query * normalizer_ref[...], heads)[:, :heads] * retain
@@ -147,12 +175,15 @@
     spread(out_ref, jnp.concatenate(parts, axis=1))
 
 
-def branch_kernel(order, whole, low, high, pieces_ref, x_ref, held_ref, got_ref, out_ref, wide_ref):
-    width = high - low
-    for at in range(pieces_ref.shape[0] // 2):
-        cols = slice(2 * width * at, 2 * width * (at + 1))
-        wide_ref[:, cols] = pair_up(pieces_ref, width, at).astype(wide_ref.dtype)
-    branch = blocks_dot(wide_ref, (held_ref, got_ref), order, whole, low, high)
+def branch_kernel(width, fetch, pieces_ref, x_ref, held_ref, got_ref, out_ref, wide_ref, *space):
+    weights = Weights(*fetch, held_ref, got_ref, *space)
+    blocks, seqs, rows = wide_ref.shape
+    count = pieces_ref.shape[0] // blocks
+    for at in range(blocks):
+        found = [pieces_ref[count * at + k][:, :width].astype(F32) for k in range(count)]
+        found.append(jnp.zeros((seqs, rows - count * width), F32))
+        wide_ref[at] = jnp.concatenate(found, axis=1).astype(wide_ref.dtype)
+    branch = weights.dot(wide_ref)
     spread(out_ref, residual_scale * x_ref[...].astype(F32) + branch)
 
 
@@ -240,18 +271,21 @@
     bf16 = stream.dtype
     copies = jax.ShapeDtypeStruct((peers, seqs, LANES), bf16)
     pair = jax.ShapeDtypeStruct((seqs, 2 * cols), bf16)
-    per_head = head_size // cols
+    pair_cols = 2 * cols
+    per_head = head_size // pair_cols
     turned = [jnp.swapaxes(w, 1, 2) for w in (query_weight, key_weight, value_weight, outgate_weight)]
-    out_turned = jnp.swapaxes(output_weight, 1, 2).reshape(-1, feats, rows // feats, cols)
-    out_turned = jnp.pad(out_turned, ((0, 0), (0, 0), (0, 0), (0, feats - cols)))
-    out_turned = out_turned.reshape(-1, feats, rows)
-
-    bulk = jnp.concatenate([w[0] for w in turned])
-    chain = jnp.concatenate([w[1] for w in turned] + [out_turned[0], out_turned[1]])[None]
+    out_turned = jnp.swapaxes(output_weight, 1, 2)
+    short = ((0, 0), (0, rows - out_turned.shape[2]))
+
+    bulk = jnp.concatenate([w[0] for w in turned] + [jnp.pad(out_turned[0], short)])
+    later = after((turned, out_turned), bulk)
+    chain = jnp.concatenate([w[1] for w in later[0]] + [jnp.pad(later[1][1], short)])[None]
+    held_in = pl.BlockSpec(memory_space=pltpu.MemorySpace.HBM)
+    here = pl.BlockSpec(memory_space=pltpu.MemorySpace.VMEM)
 
     def by_piece(x):
-        x = x.reshape(*x.shape[:-1], per_head, cols)
-        return jnp.moveaxis(x, 0, -2).reshape(*x.shape[1:-3], peers, seqs, cols)
+        x = x.reshape(*x.shape[:-1], per_head, pair_cols)
+        return jnp.moveaxis(x, 0, -2).reshape(*x.shape[1:-3], peers // 2, seqs, pair_cols)
 
     states = [by_piece(m) for m in matrix_state]
     normalizers = [by_piece(n) for n in normalizer_state]
@@ -259,37 +293,39 @@
     chips = [[2 * chip + core for chip in range(owners // 2)] for core in range(2)]
     bulk = jnp.broadcast_to(bulk, (owners // 2, *bulk.shape))
     bulk = exchange(bulk, "dp", chips)
-    got = step_of(chain, 8)
     tile = jnp.pad(stream, ((0, 0), (0, LANES - feats)))
     tile = after(tile, (*states, *normalizers, bulk))
     pieces = exchange(jnp.broadcast_to(tile, copies.shape), "tp")
     got_bulk = step_of(bulk, 1)
-    chain = merged(after(chain, (bulk,)), got)
-    got = step_of(chain, 4)
+    got = step_of(chain, 8)
     x_local = stream
     whole_x = jax.ShapeDtypeStruct((seqs, peers * feats), bf16)
     saved, new_stabs = ([], [])
     for block_no in range(gate_bias.shape[0]):
         if block_no == 0:
+            halves = (bulk, got_bulk)
+            fetch = (by_chip, False)
             x_full, qk, vo = call(
-                functools.partial(first_kernel, by_chip, 2 * cols, 4 * cols),
+                functools.partial(first_kernel, 2 * cols, (0, 4 * cols, *fetch)),
                 (whole_x, copies, pair),
                 pieces,
-                bulk,
-                got_bulk,
+                *halves,
+                specs=[here, held_in, held_in],
+                scratch=weight_space(bulk, 4 * cols),
             )
             chain = merged(after(chain, (qk,)), got)
-            got = step_of(chain, 2)
+            got = step_of(chain, 4)
         else:
-            halves = one_block((owners // 2, 4 * cols, rows))
+            halves = (chain, got)
+            fetch = (order, True)
             x_full, qk, vo = call(
-                functools.partial(norm_kernel, order, 2 * cols, 4 * cols),
+                functools.partial(norm_kernel, 2 * cols, (0, 4 * cols, *fetch)),
                 (whole_x, copies, pair),
                 pieces,
                 norm_gain[:1],
-                chain,
-                got,
-                specs=[one_block(pieces.shape), one_block((1, peers * feats)), halves, halves],
+                *halves,
+                specs=[here, here, held_in, held_in],
+                scratch=weight_space(chain, 4 * cols),
             )
             x_local = lax.dynamic_slice_in_dim(x_full, me * feats, feats, 1)
             tied = after(saved[0], (qk,))
@@ -317,20 +353,21 @@
         )
         if block_no == 0:
             chain = merged(after(chain, (hidden,)), got)
-            got = step_of(chain, 1)
+            got = step_of(chain, 2)
         saved.append((pieces, vo, retain, admit))
         pieces = exchange(hidden, "tp")
-        halves = one_block((owners // 2, feats, rows), (0, 4 * cols // feats + block_no, 0))
         summed = call(
-            functools.partial(branch_kernel, order, True, 0, feats),
+            functools.partial(branch_kernel, cols, (4 * cols, 4 * cols + feats, *fetch)),
             copies,
             pieces,
             x_local,
-            chain,
-            got,
-            scratch=[pltpu.VMEM((seqs, peers * feats), bf16)],
-            specs=[one_block(pieces.shape), one_block(x_local.shape), halves, halves],
+            *halves,
+            specs=[here, here, held_in, held_in],
+            scratch=[pltpu.VMEM((owners, seqs, rows), bf16), *weight_space(halves[0], feats)],
         )
+        if block_no == 0:
+            chain = merged(after(chain, (summed,)), got)
+            got = step_of(chain, 1)
         new_stabs.append(stab_new)
         pieces = exchange(summed, "tp")
     gain = lax.dynamic_slice_in_dim(norm_gain[1:], me * feats, feats, 1)

time: 222 us -> 235 us (1.059)
  the two profiles are of different devices: /device:TPU:14 before, /device:TPU:10 now
where the time goes in v2:
time: 235 us; the launch traced here: 233 us
  starting transfers between devices  87.3 us (37%)
  waiting for transfers between devices  63.3 us (27%)
  local copies, waits for them, and re-layouts  34.2 us (15%)
  blocking collectives  24.9 us (11%)
  Pallas kernels  16.1 us (7%)
  other arithmetic  4.29 us (2%)
    all_to_all x7, starting transfers between devices, exchange(): lax.all_to_all(pieces, axis, split_axis=0, concat_axis=0, tiled=True, axi...  69.4 us
    all_to_all x7, waiting for transfers between devices, exchange(): lax.all_to_all(pieces, axis, split_axis=0, concat_axis=0, tiled=True, axi...  63.3 us
    all_to_all x1, blocking collectives, exchange(): lax.all_to_all(pieces, axis, split_axis=0, concat_axis=0, tiled=True, axi...  24.9 us
    ppermute x5, starting transfers between devices, step_of(): return lax.ppermute(held, 'dp', [(i, i ^ bit) for i in range(size)])  17.8 us
    pallas_call x9, Pallas kernels, call(): pl.pallas_call(kernel, out_shape=out_shape, scratch_shapes=list(scratch),...  16.1 us
    unnamed x74, local copies, waits for them, and re-layouts  12.4 us
    another operation x8, local copies, waits for them, and re-layouts, by_piece(): x = x.reshape(*x.shape[:-1], per_head, pair_cols)  12.2 us
  transfers between devices with their start and end apart: 12, of which 7 were waited for; matrix products, arithmetic and copies ran while one was open for 12% of the time, Pallas kernels for 4%

profile of v2, /device:TPU:10, one launch (start us, length us, event | category | flops | bytes accessed | tf_op | source)
XLA Modules:
  0.0 233.4 jit_solution(11974586416488129572)
XLA Ops:
  4.1 16.7 %all-to-all-start = ((bf16[8,256,256]{2,1,0:T(8,128)(2,1)}), bf16[8,256,256]{2,1,0:T(8,128)(2,1)S(1)}, u32[]{:S(2)}, u32[]{:S(2)}) async-start(bf16[8,256,256]{2,1,0:T(8,128)(2,1)} %broadcast_in_dim.9), calls=%async_computation | async-start | bytes 2097152 | tf_op jit(solution)/shard_map/all_to_all | solution.py:18
  23.0 11.9 %all-to-all-done.held_ref = bf16[8,256,256]{2,1,0:T(8,128)(2,1)S(1)} async-done(((bf16[8,256,256]{2,1,0:T(8,128)(2,1)}), bf16[8,256,256]{2,1,0:T(8,128)(2,1)S(1)}, u32[]{:S(2)}, u32[]{:S(2)}) %all-to-all-start) | async-done | bytes 1048608 | tf_op jit(solution)/shard_map/all_to_all | solution.py:18
  34.9 1.9 collective-permute-start
  39.7 2.0 reshape_unstack.13
  43.0 1.7 reshape_unstack.14
  44.7 1.6 copy.20
  46.3 1.7 reshape_unstack.15
  48.0 1.7 copy.21
  52.2 24.4 %all-to-all-start.1 = ((bf16[64,8,128]{2,1,0:T(8,128)(2,1)}), bf16[64,8,128]{2,1,0:T(8,128)(2,1)}, u32[]{:S(2)}, u32[]{:S(2)}) async-start(bf16[64,8,128]{2,1,0:T(8,128)(2,1)} %broadcast_in_dim.10), calls=%async_computation.1 | async-start | bytes 262144 | tf_op jit(solution)/shard_map/all_to_all | solution.py:18
  76.6 1.4 pad_dynamic-update-slice_fusion
  78.0 6.5 %collective-permute-start.1 = (bf16[1,256,256]{2,1,0:T(8,128)(2,1)}, bf16[1,256,256]{2,1,0:T(8,128)(2,1)}, u32[]{:S(2)}, u32[]{:S(2)}) collective-permute-start(bf16[1,256,256]{2,1,0:T(8,128)(2,1)} %bitcast.26), channel_id=1, source_target_pairs={{0,8},{1,9},{2,10},{3,11},{4,12},{5,13},{6,14},{7,15},{8,0},{9,1},... | collective-permute-start | bytes 393224 | tf_op jit(solution)/shard_map/ppermute | solution.py:29
  85.0 4.7 %all-to-all-done.1.pieces_ref = bf16[64,8,128]{2,1,0:T(8,128)(2,1)} async-done(((bf16[64,8,128]{2,1,0:T(8,128)(2,1)}), bf16[64,8,128]{2,1,0:T(8,128)(2,1)}, u32[]{:S(2)}, u32[]{:S(2)}) %all-to-all-start.1) | async-done | bytes 131104 | tf_op jit(solution)/shard_map/all_to_all | solution.py:18
  89.7 2.2 shard_map.147
  93.2 8.1 %all-to-all-start.2 = ((bf16[64,8,128]{2,1,0:T(8,128)(2,1)}), bf16[64,8,128]{2,1,0:T(8,128)(2,1)}, u32[]{:S(2)}, u32[]{:S(2)}) async-start(bf16[64,8,128]{2,1,0:T(8,128)(2,1)} %copy-done.7), calls=%async_computation.2 | async-start | bytes 262144 | tf_op jit(solution)/shard_map/all_to_all | solution.py:18
  101.4 1.7 pad_maximum_fusion.2
  103.1 1.9 collective-permute-start.2
  106.9 7.0 %all-to-all-done.2.pieces_ref.refs_0_ = bf16[64,8,128]{2,1,0:T(8,128)(2,1)} async-done(((bf16[64,8,128]{2,1,0:T(8,128)(2,1)}), bf16[64,8,128]{2,1,0:T(8,128)(2,1)}, u32[]{:S(2)}, u32[]{:S(2)}) %all-to-all-start.2) | async-done | bytes 131104 | tf_op jit(solution)/shard_map/all_to_all | solution.py:18
  118.3 5.6 %collective-permute-start.3 = (bf16[4,256,256]{2,1,0:T(8,128)(2,1)S(1)}, bf16[4,256,256]{2,1,0:T(8,128)(2,1)S(1)}, u32[]{:S(2)}, u32[]{:S(2)}) collective-permute-start(bf16[4,256,256]{2,1,0:T(8,128)(2,1)S(1)} %pad_maximum_fusion.1), channel_id=1, source_target_pairs={{0,2},{1,3},{2,0},{3,1},{4,6},{5,7},{6,4},{7,5},{8,10},{9,11},{10,... | collective-permute-start | bytes 1572872 | tf_op jit(solution)/shard_map/ppermute | solution.py:29
  123.9 24.9 %all_to_all.40.pieces_ref = bf16[64,8,128]{2,1,0:T(8,128)(2,1)S(1)} all-to-all(bf16[64,8,128]{2,1,0:T(8,128)(2,1)S(1)} %shard_map.148), channel_id=1, replica_groups=mesh['tp'=64,'dp'=16] {'tp'}, dimensions={0} | all-to-all | bytes 262144 | tf_op jit(solution)/shard_map/all_to_all | solution.py:18
  149.9 1.9 collective-permute-start.4
  151.9 5.5 %all-to-all-start.4 = ((bf16[64,8,128]{2,1,0:T(8,128)(2,1)}), bf16[64,8,128]{2,1,0:T(8,128)(2,1)}, u32[]{:S(2)}, u32[]{:S(2)}) async-start(bf16[64,8,128]{2,1,0:T(8,128)(2,1)} %copy-done.6), calls=%async_computation.4 | async-start | bytes 262144 | tf_op jit(solution)/shard_map/all_to_all | solution.py:18
  157.4 1.5 fusion.16
  158.8 11.9 %all-to-all-done.4.pieces_ref = bf16[64,8,128]{2,1,0:T(8,128)(2,1)} async-done(((bf16[64,8,128]{2,1,0:T(8,128)(2,1)}), bf16[64,8,128]{2,1,0:T(8,128)(2,1)}, u32[]{:S(2)}, u32[]{:S(2)}) %all-to-all-start.4) | async-done | bytes 131104 | tf_op jit(solution)/shard_map/all_to_all | solution.py:18
  170.7 2.5 %shard_map.150 = (bf16[8,4096]{1,0:T(8,128)(2,1)S(1)}, bf16[64,8,128]{2,1,0:T(8,128)(2,1)S(1)}, bf16[8,96]{1,0:T(8,128)(2,1)S(1)}) custom-call(bf16[64,8,128]{2,1,0:T(8,128)(2,1)} %all-to-all-done.4.pieces_ref, f32[1,4096]{1,0:T(1,128)S(1)} %get-tuple-element.63.gain_ref, bf16[8,256,256]{2,1,0:T(8,128)(2,1)S(1)} %pad_maximum_fusion.held_ref, ...), custom_call_target="tpu_custom_call" | custom-call | flops 1000000 | bytes 2244608 | tf_op jit(solution)/shard_map/pallas_call | solution.py:100
  175.0 5.5 %all-to-all-start.5 = ((bf16[64,8,128]{2,1,0:T(8,128)(2,1)}), bf16[64,8,128]{2,1,0:T(8,128)(2,1)}, u32[]{:S(2)}, u32[]{:S(2)}) async-start(bf16[64,8,128]{2,1,0:T(8,128)(2,1)} %copy-done.8), calls=%async_computation.5 | async-start | bytes 262144 | tf_op jit(solution)/shard_map/all_to_all | solution.py:18
  182.4 10.7 %all-to-all-done.5.pieces_ref.refs_0_ = bf16[64,8,128]{2,1,0:T(8,128)(2,1)} async-done(((bf16[64,8,128]{2,1,0:T(8,128)(2,1)}), bf16[64,8,128]{2,1,0:T(8,128)(2,1)}, u32[]{:S(2)}, u32[]{:S(2)}) %all-to-all-start.5) | async-done | bytes 131104 | tf_op jit(solution)/shard_map/all_to_all | solution.py:18
  196.7 4.6 %all-to-all-start.6 = ((bf16[64,8,128]{2,1,0:T(8,128)(2,1)}), bf16[64,8,128]{2,1,0:T(8,128)(2,1)S(1)}, u32[]{:S(2)}, u32[]{:S(2)}) async-start(bf16[64,8,128]{2,1,0:T(8,128)(2,1)} %copy-done.5), calls=%async_computation.6 | async-start | bytes 262144 | tf_op jit(solution)/shard_map/all_to_all | solution.py:18
  202.0 12.0 %all-to-all-done.6.pieces_ref = bf16[64,8,128]{2,1,0:T(8,128)(2,1)S(1)} async-done(((bf16[64,8,128]{2,1,0:T(8,128)(2,1)}), bf16[64,8,128]{2,1,0:T(8,128)(2,1)S(1)}, u32[]{:S(2)}, u32[]{:S(2)}) %all-to-all-start.6) | async-done | bytes 131104 | tf_op jit(solution)/shard_map/all_to_all | solution.py:18
  215.2 4.6 %all-to-all-start.7 = ((bf16[64,8,128]{2,1,0:T(8,128)(2,1)}), bf16[64,8,128]{2,1,0:T(8,128)(2,1)S(1)}, u32[]{:S(2)}, u32[]{:S(2)}) async-start(bf16[64,8,128]{2,1,0:T(8,128)(2,1)} %shard_map.152), calls=%async_computation.7 | async-start | bytes 262144 | tf_op jit(solution)/shard_map/all_to_all | solution.py:18
  220.6 3.1 %shard_map.154 = (f32[2,8,3,16,192]{4,3,2,1,0:T(8,128)}, f32[2,8,16,192]{3,2,1,0:T(8,128)}) custom-call(bf16[64,8,128]{2,1,0:T(8,128)(2,1)} %all-to-all-done.2.pieces_ref.refs_0_, bf16[8,96]{1,0:T(8,128)(2,1)S(1)} %copy-done.17, f32[8,16]{1,0:T(8,128)S(1)} %copy-done.15, f32[8,16]{1,0:T(8,128)S(1)} %copy-done.13, f32[2,8,3,16,192]{4,3,2,1,0:T(8,128)S(1)} %copy-done, ...), custom_call_target="tpu_custom_call" | custom-call | flops 1000000 | bytes 920064 | tf_op jit(solution)/shard_map/pallas_call | solution.py:100
  224.3 3.1 %shard_map.155 = (f32[2,8,3,16,192]{4,3,2,1,0:T(8,128)}, f32[2,8,16,192]{3,2,1,0:T(8,128)}) custom-call(bf16[64,8,128]{2,1,0:T(8,128)(2,1)} %all-to-all-done.5.pieces_ref.refs_0_, bf16[8,96]{1,0:T(8,128)(2,1)S(1)} %copy-done.19, f32[8,16]{1,0:T(8,128)S(1)} %get-tuple-element.48.retain_ref.refs_2_, ...), custom_call_target="tpu_custom_call", output_to_operand_aliasing={{0}: (6, {}), {1}: (7, {})} | custom-call | flops 1000000 | bytes 1706496 | tf_op jit(solution)/shard_map/pallas_call | solution.py:100
  227.4 5.1 %all-to-all-done.7.pieces_ref = bf16[64,8,128]{2,1,0:T(8,128)(2,1)S(1)} async-done(((bf16[64,8,128]{2,1,0:T(8,128)(2,1)}), bf16[64,8,128]{2,1,0:T(8,128)(2,1)S(1)}, u32[]{:S(2)}, u32[]{:S(2)}) %all-to-all-start.7) | async-done | bytes 131104 | tf_op jit(solution)/shard_map/all_to_all | solution.py:18
  (105 shorter events, 32.8 us)
Async XLA Ops:
  0.6 1.5 copy-start.23
  4.1 16.7 %copy-start.22 = (bf16[2,256,48]{1,2,0:T(8,128)(2,1)S(1)}, bf16[2,256,48]{1,2,0:T(8,128)(2,1)}, u32[]{:S(2)}) copy-start(bf16[2,256,48]{1,2,0:T(8,128)(2,1)} %param.13) | copy-start | bytes 147460
  4.1 17.3 %copy-start.1 = (f32[2,8,16,192]{3,2,1,0:T(8,128)S(1)}, f32[2,8,16,192]{3,2,1,0:T(8,128)}, u32[]{:S(2)}) copy-start(f32[2,8,16,192]{3,2,1,0:T(8,128)} %refs_5_.3) | copy-start | bytes 589828
  4.1 18.0 %copy-start = (f32[2,8,3,16,192]{4,3,2,1,0:T(8,128)S(1)}, f32[2,8,3,16,192]{4,3,2,1,0:T(8,128)}, u32[]{:S(2)}) copy-start(f32[2,8,3,16,192]{4,3,2,1,0:T(8,128)} %refs_4_.3) | copy-start | bytes 1769476
  4.1 30.8 %all-to-all-start = ((bf16[8,256,256]{2,1,0:T(8,128)(2,1)}), bf16[8,256,256]{2,1,0:T(8,128)(2,1)S(1)}, u32[]{:S(2)}, u32[]{:S(2)}) async-start(bf16[8,256,256]{2,1,0:T(8,128)(2,1)} %broadcast_in_dim.9), calls=%async_computation | async-start | bytes 2097152 | tf_op jit(solution)/shard_map/all_to_all | solution.py:18
  34.9 54.8 %collective-permute-start = (bf16[8,256,256]{2,1,0:T(8,128)(2,1)S(1)}, bf16[8,256,256]{2,1,0:T(8,128)(2,1)S(1)}, u32[]{:S(2)}, u32[]{:S(2)}) collective-permute-start(bf16[8,256,256]{2,1,0:T(8,128)(2,1)S(1)} %all-to-all-done.held_ref), channel_id=1, source_target_pairs={{0,1},{1,0},{2,3},{3,2},{4,5},{5,4},{6,7},{7,6},{8,9},{9,8},{10,11... | collective-permute-start | bytes 3145736 | tf_op jit(solution)/shard_map/ppermute | solution.py:29
  48.0 1.7 copy-start.20
  48.0 1.7 copy-start.25
  48.0 2.3 copy-start.27
  49.6 1.2 copy-start.21
  52.2 37.5 %all-to-all-start.1 = ((bf16[64,8,128]{2,1,0:T(8,128)(2,1)}), bf16[64,8,128]{2,1,0:T(8,128)(2,1)}, u32[]{:S(2)}, u32[]{:S(2)}) async-start(bf16[64,8,128]{2,1,0:T(8,128)(2,1)} %broadcast_in_dim.10), calls=%async_computation.1 | async-start | bytes 262144 | tf_op jit(solution)/shard_map/all_to_all | solution.py:18
  78.0 6.5 %copy-start.32 = (f32[2,32]{1,0:T(2,128)S(1)}, f32[2,32]{1,0:T(2,128)}, u32[]{:S(2)}) copy-start(f32[2,32]{1,0:T(2,128)} %param.18) | copy-start | bytes 772
  78.0 23.4 %collective-permute-start.1 = (bf16[1,256,256]{2,1,0:T(8,128)(2,1)}, bf16[1,256,256]{2,1,0:T(8,128)(2,1)}, u32[]{:S(2)}, u32[]{:S(2)}) collective-permute-start(bf16[1,256,256]{2,1,0:T(8,128)(2,1)} %bitcast.26), channel_id=1, source_target_pairs={{0,8},{1,9},{2,10},{3,11},{4,12},{5,13},{6,14},{7,15},{8,0},{9,1},... | collective-permute-start | bytes 393224 | tf_op jit(solution)/shard_map/ppermute | solution.py:29
  93.2 20.7 %copy-start.16 = (bf16[8,96]{1,0:T(8,128)(2,1)}, bf16[8,96]{1,0:T(8,128)(2,1)S(1)}, u32[]{:S(2)}) copy-start(bf16[8,96]{1,0:T(8,128)(2,1)S(1)} %get-tuple-element.51.vo_ref.refs_1_) | copy-start | bytes 4612
  93.2 20.7 %all-to-all-start.2 = ((bf16[64,8,128]{2,1,0:T(8,128)(2,1)}), bf16[64,8,128]{2,1,0:T(8,128)(2,1)}, u32[]{:S(2)}, u32[]{:S(2)}) async-start(bf16[64,8,128]{2,1,0:T(8,128)(2,1)} %copy-done.7), calls=%async_computation.2 | async-start | bytes 262144 | tf_op jit(solution)/shard_map/all_to_all | solution.py:18
  101.4 3.7 %copy-start.11 = (bf16[8,4096]{1,0:T(8,128)(2,1)S(1)}, bf16[8,4096]{1,0:T(8,128)(2,1)}, u32[]{:S(2)}) copy-start(bf16[8,4096]{1,0:T(8,128)(2,1)} %copy-done.10) | copy-start | bytes 196612
  103.1 14.0 %collective-permute-start.2 = (bf16[2,256,256]{2,1,0:T(8,128)(2,1)}, bf16[2,256,256]{2,1,0:T(8,128)(2,1)}, u32[]{:S(2)}, u32[]{:S(2)}) collective-permute-start(bf16[2,256,256]{2,1,0:T(8,128)(2,1)} %pad_maximum_fusion.2), channel_id=1, source_target_pairs={{0,4},{1,5},{2,6},{3,7},{4,0},{5,1},{6,2},{7,3},{8,12},{9,13},{10,... | collective-permute-start | bytes 786440 | tf_op jit(solution)/shard_map/ppermute | solution.py:29
  105.1 1.1 copy-start.29
  106.9 10.3 %copy-start.12 = (f32[8,16]{1,0:T(8,128)}, f32[8,16]{1,0:T(8,128)S(1)}, u32[]{:S(2)}) copy-start(f32[8,16]{1,0:T(8,128)S(1)} %get-tuple-element.53.admit_ref.refs_3_) | copy-start | bytes 1540
  106.9 10.3 %copy-start.14 = (f32[8,16]{1,0:T(8,128)}, f32[8,16]{1,0:T(8,128)S(1)}, u32[]{:S(2)}) copy-start(f32[8,16]{1,0:T(8,128)S(1)} %get-tuple-element.52.retain_ref.refs_2_) | copy-start | bytes 1540
  113.9 1.0 copy-start.2
  114.9 0.9 copy-start.4
  118.3 31.0 %collective-permute-start.3 = (bf16[4,256,256]{2,1,0:T(8,128)(2,1)S(1)}, bf16[4,256,256]{2,1,0:T(8,128)(2,1)S(1)}, u32[]{:S(2)}, u32[]{:S(2)}) collective-permute-start(bf16[4,256,256]{2,1,0:T(8,128)(2,1)S(1)} %pad_maximum_fusion.1), channel_id=1, source_target_pairs={{0,2},{1,3},{2,0},{3,1},{4,6},{5,7},{6,4},{7,5},{8,10},{9,11},{10,... | collective-permute-start | bytes 1572872 | tf_op jit(solution)/shard_map/ppermute | solution.py:29
  149.9 20.7 %collective-permute-start.4 = (bf16[8,256,256]{2,1,0:T(8,128)(2,1)S(1)}, bf16[8,256,256]{2,1,0:T(8,128)(2,1)S(1)}, u32[]{:S(2)}, u32[]{:S(2)}) collective-permute-start(bf16[8,256,256]{2,1,0:T(8,128)(2,1)S(1)} %pad_maximum_fusion.held_ref), channel_id=1, source_target_pairs={{0,1},{1,0},{2,3},{3,2},{4,5},{5,4},{6,7},{7,6},{8,9},{9,8},{10,11... | collective-permute-start | bytes 3145736 | tf_op jit(solution)/shard_map/ppermute | solution.py:29
  151.9 18.8 %all-to-all-start.4 = ((bf16[64,8,128]{2,1,0:T(8,128)(2,1)}), bf16[64,8,128]{2,1,0:T(8,128)(2,1)}, u32[]{:S(2)}, u32[]{:S(2)}) async-start(bf16[64,8,128]{2,1,0:T(8,128)(2,1)} %copy-done.6), calls=%async_computation.4 | async-start | bytes 262144 | tf_op jit(solution)/shard_map/all_to_all | solution.py:18
  175.0 18.1 %all-to-all-start.5 = ((bf16[64,8,128]{2,1,0:T(8,128)(2,1)}), bf16[64,8,128]{2,1,0:T(8,128)(2,1)}, u32[]{:S(2)}, u32[]{:S(2)}) async-start(bf16[64,8,128]{2,1,0:T(8,128)(2,1)} %copy-done.8), calls=%async_computation.5 | async-start | bytes 262144 | tf_op jit(solution)/shard_map/all_to_all | solution.py:18
  181.1 1.2 copy-start.30
  196.7 17.4 %all-to-all-start.6 = ((bf16[64,8,128]{2,1,0:T(8,128)(2,1)}), bf16[64,8,128]{2,1,0:T(8,128)(2,1)S(1)}, u32[]{:S(2)}, u32[]{:S(2)}) async-start(bf16[64,8,128]{2,1,0:T(8,128)(2,1)} %copy-done.5), calls=%async_computation.6 | async-start | bytes 262144 | tf_op jit(solution)/shard_map/all_to_all | solution.py:18
  215.2 5.4 %copy-start.13 = (f32[8,16]{1,0:T(8,128)S(1)}, f32[8,16]{1,0:T(8,128)}, u32[]{:S(2)}) copy-start(f32[8,16]{1,0:T(8,128)} %copy-done.12) | copy-start | bytes 1540
  215.2 5.4 %copy-start.15 = (f32[8,16]{1,0:T(8,128)S(1)}, f32[8,16]{1,0:T(8,128)}, u32[]{:S(2)}) copy-start(f32[8,16]{1,0:T(8,128)} %copy-done.14) | copy-start | bytes 1540
  215.2 17.3 %all-to-all-start.7 = ((bf16[64,8,128]{2,1,0:T(8,128)(2,1)}), bf16[64,8,128]{2,1,0:T(8,128)(2,1)S(1)}, u32[]{:S(2)}, u32[]{:S(2)}) async-start(bf16[64,8,128]{2,1,0:T(8,128)(2,1)} %shard_map.152), calls=%async_computation.7 | async-start | bytes 262144 | tf_op jit(solution)/shard_map/all_to_all | solution.py:18
  220.6 3.1 %copy-start.28 = (f32[1,8,16]{2,1,0:T(8,128)S(1)}, f32[1,8,16]{2,1,0:T(8,128)}, u32[]{:S(2)}) copy-start(f32[1,8,16]{2,1,0:T(8,128)} %get-tuple-element.64) | copy-start | bytes 1540
  (13 other events, 9.0 us)

commit v3 on v2

--- a/solution.py
+++ b/solution.py
@@ -14,10 +14,8 @@
 F32 = jnp.float32
 
 
-def exchange(pieces, axis, groups=None):
-    return lax.all_to_all(
-        pieces, axis, split_axis=0, concat_axis=0, tiled=True, axis_index_groups=groups
-    )
+def exchange(pieces, axis):
+    return lax.all_to_all(pieces, axis, split_axis=0, concat_axis=0, tiled=True)
 
 
 def after(x, earlier):
@@ -113,13 +111,42 @@
     return pl.BlockSpec(shape, lambda step: at)
 
 
-def first_kernel(cut, fetch, pieces_ref, held_ref, got_ref, x_ref, qk_ref, vo_ref, *space):
-    weights = Weights(*fetch, held_ref, got_ref, *space)
+def pack_kernel(*refs):
+    *project_refs, output_ref, own_ref, chain_ref = refs
+    at = 0
+    for ref in project_refs:
+        size = ref.shape[1]
+        own_ref[at : at + size, :] = ref[0]
+        chain_ref[0, at : at + size, :] = ref[1]
+        at += size
+    blocks, size, rows = output_ref.shape
+    for block in range(blocks):
+        chain_ref[0, at : at + size, :rows] = output_ref[block]
+        chain_ref[0, at : at + size, rows:] = jnp.zeros(
+            (size, chain_ref.shape[2] - rows), chain_ref.dtype
+        )
+        at += size
+
+
+def whole_kernel(pieces_ref, x_ref, cut_ref):
     width = x_ref.shape[1] // pieces_ref.shape[0]
+    rows = cut_ref.shape[2]
     for at in range(pieces_ref.shape[0] // 2):
-        cols = slice(2 * width * at, 2 * width * (at + 1))
-        x_ref[:, cols] = pair_up(pieces_ref, width, at).astype(x_ref.dtype)
-    out = weights.dot(x_ref)
+        low = 2 * width * at
+        pair = pair_up(pieces_ref, width, at).astype(x_ref.dtype)
+        x_ref[:, low : low + 2 * width] = pair
+        cut_ref[low // rows, :, low % rows : low % rows + 2 * width] = pair
+
+
+def partial_kernel(x_ref, weight_ref, out_ref):
+    owners, seqs, rows = x_ref.shape
+    x = x_ref[...].reshape(owners * seqs, rows)
+    out = row_dot(x, weight_ref[...])
+    out_ref[...] = out.reshape(out_ref.shape).astype(out_ref.dtype)
+
+
+def sum_kernel(cut, parts_ref, qk_ref, vo_ref):
+    out = sum(parts_ref[at].astype(F32) for at in range(parts_ref.shape[0]))
     spread(qk_ref, out[:, :cut])
     vo_ref[...] = out[:, cut:].astype(vo_ref.dtype)
 
@@ -266,7 +293,6 @@
     peers = lax.axis_size("tp")
     owners = lax.axis_size("dp")
     order = chain_order(owners)
-    by_chip = [2 * chip for chip in range(owners // 2)]
     me = lax.axis_index("tp")
     bf16 = stream.dtype
     copies = jax.ShapeDtypeStruct((peers, seqs, LANES), bf16)
@@ -275,13 +301,17 @@
     per_head = head_size // pair_cols
     turned = [jnp.swapaxes(w, 1, 2) for w in (query_weight, key_weight, value_weight, outgate_weight)]
     out_turned = jnp.swapaxes(output_weight, 1, 2)
-    short = ((0, 0), (0, rows - out_turned.shape[2]))
-
-    bulk = jnp.concatenate([w[0] for w in turned] + [jnp.pad(out_turned[0], short)])
-    later = after((turned, out_turned), bulk)
-    chain = jnp.concatenate([w[1] for w in later[0]] + [jnp.pad(later[1][1], short)])[None]
     held_in = pl.BlockSpec(memory_space=pltpu.MemorySpace.HBM)
     here = pl.BlockSpec(memory_space=pltpu.MemorySpace.VMEM)
+    own, chain = call(
+        pack_kernel,
+        (
+            jax.ShapeDtypeStruct((4 * cols, rows), bf16),
+            jax.ShapeDtypeStruct((1, 4 * cols + 2 * feats, rows), bf16),
+        ),
+        *turned,
+        out_turned,
+    )
 
     def by_piece(x):
         x = x.reshape(*x.shape[:-1], per_head, pair_cols)
@@ -290,40 +320,36 @@
     states = [by_piece(m) for m in matrix_state]
     normalizers = [by_piece(n) for n in normalizer_state]
 
-    chips = [[2 * chip + core for chip in range(owners // 2)] for core in range(2)]
-    bulk = jnp.broadcast_to(bulk, (owners // 2, *bulk.shape))
-    bulk = exchange(bulk, "dp", chips)
+    whole_x = jax.ShapeDtypeStruct((seqs, peers * feats), bf16)
     tile = jnp.pad(stream, ((0, 0), (0, LANES - feats)))
-    tile = after(tile, (*states, *normalizers, bulk))
     pieces = exchange(jnp.broadcast_to(tile, copies.shape), "tp")
-    got_bulk = step_of(bulk, 1)
     got = step_of(chain, 8)
     x_local = stream
-    whole_x = jax.ShapeDtypeStruct((seqs, peers * feats), bf16)
+    x_full, cut = call(
+        whole_kernel, (whole_x, jax.ShapeDtypeStruct((owners, seqs, rows), bf16)), pieces
+    )
+    everyone = exchange(cut, "dp")
+    partial = call(
+        partial_kernel, jax.ShapeDtypeStruct((owners, seqs, 4 * cols), bf16), everyone, own
+    )
+    partial = after(partial, (states, normalizers))
+    parts = exchange(partial, "dp")
+    chain = merged(after(chain, (partial,)), got)
+    got = step_of(chain, 4)
     saved, new_stabs = ([], [])
     for block_no in range(gate_bias.shape[0]):
         if block_no == 0:
-            halves = (bulk, got_bulk)
-            fetch = (by_chip, False)
+            qk, vo = call(functools.partial(sum_kernel, 2 * cols), (copies, pair), parts)
+            chain = merged(after(chain, (qk,)), got)
+            got = step_of(chain, 2)
+        else:
             x_full, qk, vo = call(
-                functools.partial(first_kernel, 2 * cols, (0, 4 * cols, *fetch)),
-                (whole_x, copies, pair),
-                pieces,
-                *halves,
-                specs=[here, held_in, held_in],
-                scratch=weight_space(bulk, 4 * cols),
-            )
-            chain = merged(after(chain, (qk,)), got)
-            got = step_of(chain, 4)
-        else:
-            halves = (chain, got)
-            fetch = (order, True)
-            x_full, qk, vo = call(
-                functools.partial(norm_kernel, 2 * cols, (0, 4 * cols, *fetch)),
+                functools.partial(norm_kernel, 2 * cols, (0, 4 * cols, order, True)),
                 (whole_x, copies, pair),
                 pieces,
                 norm_gain[:1],
-                *halves,
+                chain,
+                got,
                 specs=[here, here, held_in, held_in],
                 scratch=weight_space(chain, 4 * cols),
             )
@@ -353,21 +379,20 @@
         )
         if block_no == 0:
             chain = merged(after(chain, (hidden,)), got)
-            got = step_of(chain, 2)
+            got = step_of(chain, 1)
         saved.append((pieces, vo, retain, admit))
         pieces = exchange(hidden, "tp")
+        low = 4 * cols + block_no * feats
         summed = call(
-            functools.partial(branch_kernel, cols, (4 * cols, 4 * cols + feats, *fetch)),
+            functools.partial(branch_kernel, cols, (low, low + feats, order, True)),
             copies,
             pieces,
             x_local,
-            *halves,
+            chain,
+            got,
             specs=[here, here, held_in, held_in],
-            scratch=[pltpu.VMEM((owners, seqs, rows), bf16), *weight_space(halves[0], feats)],
+            scratch=[pltpu.VMEM((owners, seqs, rows), bf16), *weight_space(chain, feats)],
         )
-        if block_no == 0:
-            chain = merged(after(chain, (summed,)), got)
-            got = step_of(chain, 1)
         new_stabs.append(stab_new)
         pieces = exchange(summed, "tp")
     gain = lax.dynamic_slice_in_dim(norm_gain[1:], me * feats, feats, 1)

time: 235 us -> 199 us (0.85)
  the two profiles are of different devices: /device:TPU:10 before, /device:TPU:2 now
where the time goes in v3:
time: 199 us; the launch traced here: 198 us
  starting transfers between devices  73.8 us (37%)
  waiting for transfers between devices  57 us (29%)
  blocking collectives  35.6 us (18%)
  local copies, waits for them, and re-layouts  13.1 us (7%)
  Pallas kernels  13.1 us (7%)
  matrix products  2.24 us (1%)
  other arithmetic  2.21 us (1%)
    all_to_all x7, starting transfers between devices, exchange(): return lax.all_to_all(pieces, axis, split_axis=0, concat_axis=0, tiled=True)  59.4 us
    all_to_all x7, waiting for transfers between devices, exchange(): return lax.all_to_all(pieces, axis, split_axis=0, concat_axis=0, tiled=True)  57 us
    all_to_all x2, blocking collectives, exchange(): return lax.all_to_all(pieces, axis, split_axis=0, concat_axis=0, tiled=True)  35.6 us
    ppermute x4, starting transfers between devices, step_of(): return lax.ppermute(held, 'dp', [(i, i ^ bit) for i in range(size)])  14.4 us
    pallas_call x12, Pallas kernels, call(): pl.pallas_call(kernel, out_shape=out_shape, scratch_shapes=list(scratch),...  13.1 us
    unnamed x44, local copies, waits for them, and re-layouts  7.03 us
  transfers between devices with their start and end apart: 11, of which 7 were waited for; matrix products, arithmetic and copies ran while one was open for 4% of the time, Pallas kernels for 3%

profile of v3, /device:TPU:2, one launch (start us, length us, event | category | flops | bytes accessed | tf_op | source)
XLA Modules:
  0.0 198.1 jit_solution(12387312029650203560)
XLA Ops:
  2.0 23.4 %all-to-all-start = ((bf16[64,8,128]{2,1,0:T(8,128)(2,1)}), bf16[64,8,128]{2,1,0:T(8,128)(2,1)S(1)}, u32[]{:S(2)}, u32[]{:S(2)}) async-start(bf16[64,8,128]{2,1,0:T(8,128)(2,1)} %broadcast_in_dim.3), calls=%async_computation | async-start | bytes 262144 | tf_op jit(solution)/shard_map/all_to_all | solution.py:18
  25.5 0.8 copy-done.6
  29.5 6.5 %collective-permute-start = (bf16[1,320,256]{2,1,0:T(8,128)(2,1)S(1)}, bf16[1,320,256]{2,1,0:T(8,128)(2,1)S(1)}, u32[]{:S(2)}, u32[]{:S(2)}) collective-permute-start(bf16[1,320,256]{2,1,0:T(8,128)(2,1)S(1)} %get-tuple-element.36), channel_id=1, source_target_pairs={{0,8},{1,9},{2,10},{3,11},{4,12},{5,13},{6,14},{7,15},{8,0},{9,1},... | collective-permute-start | bytes 491528 | tf_op jit(solution)/shard_map/ppermute | solution.py:27
  36.0 1.2 fusion.10
  37.2 1.0 all-to-all-done.pieces_ref
  38.9 7.3 %all-to-all-start.1 = ((bf16[16,8,256]{2,1,0:T(8,128)(2,1)}), bf16[16,8,256]{2,1,0:T(8,128)(2,1)S(1)}, u32[]{:S(2)}, u32[]{:S(2)}) async-start(bf16[16,8,256]{2,1,0:T(8,128)(2,1)} %get-tuple-element.29), calls=%async_computation.1 | async-start | bytes 131072 | tf_op jit(solution)/shard_map/all_to_all | solution.py:18
  47.7 5.0 %all-to-all-done.1.x_ref = bf16[16,8,256]{2,1,0:T(8,128)(2,1)S(1)} async-done(((bf16[16,8,256]{2,1,0:T(8,128)(2,1)}), bf16[16,8,256]{2,1,0:T(8,128)(2,1)S(1)}, u32[]{:S(2)}, u32[]{:S(2)}) %all-to-all-start.1) | async-done | bytes 65568 | tf_op jit(solution)/shard_map/all_to_all | solution.py:18
  52.9 2.7 %collective-permute-start.1 = (bf16[2,320,256]{2,1,0:T(8,128)(2,1)S(1)}, bf16[2,320,256]{2,1,0:T(8,128)(2,1)S(1)}, u32[]{:S(2)}, u32[]{:S(2)}) collective-permute-start(bf16[2,320,256]{2,1,0:T(8,128)(2,1)S(1)} %pad_maximum_fusion.2), channel_id=1, source_target_pairs={{0,4},{1,5},{2,6},{3,7},{4,0},{5,1},{6,2},{7,3},{8,12},{9,13},{10,... | collective-permute-start | bytes 983048 | tf_op jit(solution)/shard_map/ppermute | solution.py:27
  55.7 18.3 %all_to_all.45.parts_ref = bf16[16,8,192]{2,1,0:T(8,128)(2,1)S(1)} all-to-all(bf16[16,8,192]{2,1,0:T(8,128)(2,1)S(1)} %shard_map.149), channel_id=1, replica_groups=mesh['tp'=64,'dp'=16] {'dp'}, dimensions={0} | all-to-all | bytes 98304 | tf_op jit(solution)/shard_map/all_to_all | solution.py:18
  74.7 3.3 %collective-permute-start.2 = (bf16[4,320,256]{2,1,0:T(8,128)(2,1)S(1)}, bf16[4,320,256]{2,1,0:T(8,128)(2,1)S(1)}, u32[]{:S(2)}, u32[]{:S(2)}) collective-permute-start(bf16[4,320,256]{2,1,0:T(8,128)(2,1)S(1)} %pad_maximum_fusion.1), channel_id=1, source_target_pairs={{0,2},{1,3},{2,0},{3,1},{4,6},{5,7},{6,4},{7,5},{8,10},{9,11},{10,... | collective-permute-start | bytes 1966088 | tf_op jit(solution)/shard_map/ppermute | solution.py:27
  78.0 9.2 %all-to-all-start.3 = ((bf16[64,8,128]{2,1,0:T(8,128)(2,1)}), bf16[64,8,128]{2,1,0:T(8,128)(2,1)S(1)}, u32[]{:S(2)}, u32[]{:S(2)}) async-start(bf16[64,8,128]{2,1,0:T(8,128)(2,1)} %get-tuple-element.32), calls=%async_computation.3 | async-start | bytes 262144 | tf_op jit(solution)/shard_map/all_to_all | solution.py:18
  87.3 1.1 convolution_add_fusion.1
  89.1 10.9 %all-to-all-done.3.pieces_ref.refs_0_ = bf16[64,8,128]{2,1,0:T(8,128)(2,1)S(1)} async-done(((bf16[64,8,128]{2,1,0:T(8,128)(2,1)}), bf16[64,8,128]{2,1,0:T(8,128)(2,1)S(1)}, u32[]{:S(2)}, u32[]{:S(2)}) %all-to-all-start.3) | async-done | bytes 131104 | tf_op jit(solution)/shard_map/all_to_all | solution.py:18
  100.5 1.9 collective-permute-start.3
  102.5 17.3 %all_to_all.46.pieces_ref = bf16[64,8,128]{2,1,0:T(8,128)(2,1)S(1)} all-to-all(bf16[64,8,128]{2,1,0:T(8,128)(2,1)S(1)} %shard_map.151), channel_id=1, replica_groups=mesh['tp'=64,'dp'=16] {'tp'}, dimensions={0} | all-to-all | bytes 262144 | tf_op jit(solution)/shard_map/all_to_all | solution.py:18
  119.8 1.2 shard_map.152
  121.0 4.6 %all-to-all-start.5 = ((bf16[64,8,128]{2,1,0:T(8,128)(2,1)}), bf16[64,8,128]{2,1,0:T(8,128)(2,1)S(1)}, u32[]{:S(2)}, u32[]{:S(2)}) async-start(bf16[64,8,128]{2,1,0:T(8,128)(2,1)} %shard_map.152), calls=%async_computation.5 | async-start | bytes 262144 | tf_op jit(solution)/shard_map/all_to_all | solution.py:18
  126.2 12.1 %all-to-all-done.5.pieces_ref = bf16[64,8,128]{2,1,0:T(8,128)(2,1)S(1)} async-done(((bf16[64,8,128]{2,1,0:T(8,128)(2,1)}), bf16[64,8,128]{2,1,0:T(8,128)(2,1)S(1)}, u32[]{:S(2)}, u32[]{:S(2)}) %all-to-all-start.5) | async-done | bytes 131104 | tf_op jit(solution)/shard_map/all_to_all | solution.py:18
  138.4 2.1 %shard_map.153 = (bf16[8,4096]{1,0:T(8,128)(2,1)S(1)}, bf16[64,8,128]{2,1,0:T(8,128)(2,1)}, bf16[8,96]{1,0:T(8,128)(2,1)S(1)}) custom-call(bf16[64,8,128]{2,1,0:T(8,128)(2,1)S(1)} %all-to-all-done.5.pieces_ref, f32[1,4096]{1,0:T(1,128)S(1)} %get-tuple-element.59.gain_ref, bf16[8,320,256]{2,1,0:T(8,128)(2,1)S(1)} %pad_maximum_fusion.held_ref, ...), custom_call_target="tpu_custom_call" | custom-call | flops 1000000 | bytes 2768896 | tf_op jit(solution)/shard_map/pallas_call | solution.py:98
  140.5 4.6 %all-to-all-start.6 = ((bf16[64,8,128]{2,1,0:T(8,128)(2,1)}), bf16[64,8,128]{2,1,0:T(8,128)(2,1)S(1)}, u32[]{:S(2)}, u32[]{:S(2)}) async-start(bf16[64,8,128]{2,1,0:T(8,128)(2,1)} %get-tuple-element.39), calls=%async_computation.6 | async-start | bytes 262144 | tf_op jit(solution)/shard_map/all_to_all | solution.py:18
  145.2 1.1 convolution_add_fusion
  147.0 10.9 %all-to-all-done.6.pieces_ref.refs_0_ = bf16[64,8,128]{2,1,0:T(8,128)(2,1)S(1)} async-done(((bf16[64,8,128]{2,1,0:T(8,128)(2,1)}), bf16[64,8,128]{2,1,0:T(8,128)(2,1)S(1)}, u32[]{:S(2)}, u32[]{:S(2)}) %all-to-all-start.6) | async-done | bytes 131104 | tf_op jit(solution)/shard_map/all_to_all | solution.py:18
  157.9 1.1 shard_map.154
  159.0 5.5 %all-to-all-start.7 = ((bf16[64,8,128]{2,1,0:T(8,128)(2,1)}), bf16[64,8,128]{2,1,0:T(8,128)(2,1)}, u32[]{:S(2)}, u32[]{:S(2)}) async-start(bf16[64,8,128]{2,1,0:T(8,128)(2,1)} %shard_map.154), calls=%async_computation.7 | async-start | bytes 262144 | tf_op jit(solution)/shard_map/all_to_all | solution.py:18
  165.1 11.8 %all-to-all-done.7.pieces_ref = bf16[64,8,128]{2,1,0:T(8,128)(2,1)} async-done(((bf16[64,8,128]{2,1,0:T(8,128)(2,1)}), bf16[64,8,128]{2,1,0:T(8,128)(2,1)}, u32[]{:S(2)}, u32[]{:S(2)}) %all-to-all-start.7) | async-done | bytes 131104 | tf_op jit(solution)/shard_map/all_to_all | solution.py:18
  177.6 1.4 shard_map.155
  179.7 4.7 %all-to-all-start.8 = ((bf16[64,8,128]{2,1,0:T(8,128)(2,1)}), bf16[64,8,128]{2,1,0:T(8,128)(2,1)S(1)}, u32[]{:S(2)}, u32[]{:S(2)}) async-start(bf16[64,8,128]{2,1,0:T(8,128)(2,1)} %copy-done.5), calls=%async_computation.8 | async-start | bytes 262144 | tf_op jit(solution)/shard_map/all_to_all | solution.py:18
  185.2 0.9 copy-done.2
  186.8 2.2 %shard_map.157 = (f32[2,8,3,16,192]{4,3,2,1,0:T(8,128)}, f32[2,8,16,192]{3,2,1,0:T(8,128)}) custom-call(bf16[64,8,128]{2,1,0:T(8,128)(2,1)S(1)} %all-to-all-done.3.pieces_ref.refs_0_, bf16[8,96]{1,0:T(8,128)(2,1)S(1)} %copy-done.12, f32[8,16]{1,0:T(8,128)S(1)} %get-tuple-element.48.retain_ref.refs_2_, f32[8,16]{1,0:T(8,128)S(1)} %get-tuple-element.49.admit_ref.refs_3_, ...), custom_call_target="tpu_custom_call" | custom-call | flops 1000000 | bytes 920064 | tf_op jit(solution)/shard_map/pallas_call | solution.py:98
  189.7 2.2 %shard_map.158 = (f32[2,8,3,16,192]{4,3,2,1,0:T(8,128)}, f32[2,8,16,192]{3,2,1,0:T(8,128)}) custom-call(bf16[64,8,128]{2,1,0:T(8,128)(2,1)S(1)} %copy-done.4, bf16[8,96]{1,0:T(8,128)(2,1)S(1)} %copy-done.14, f32[8,16]{1,0:T(8,128)S(1)} %get-tuple-element.44.retain_ref.refs_2_, ...), custom_call_target="tpu_custom_call", output_to_operand_aliasing={{0}: (6, {}), {1}: (7, {})} | custom-call | flops 1000000 | bytes 1706496 | tf_op jit(solution)/shard_map/pallas_call | solution.py:98
  191.9 5.3 %all-to-all-done.8.pieces_ref = bf16[64,8,128]{2,1,0:T(8,128)(2,1)S(1)} async-done(((bf16[64,8,128]{2,1,0:T(8,128)(2,1)}), bf16[64,8,128]{2,1,0:T(8,128)(2,1)S(1)}, u32[]{:S(2)}, u32[]{:S(2)}) %all-to-all-start.8) | async-done | bytes 131104 | tf_op jit(solution)/shard_map/all_to_all | solution.py:18
  197.2 0.9 shard_map.156
  (72 shorter events, 14.4 us)
Async XLA Ops:
  0.6 45.6 %copy-start.1 = (f32[2,8,16,192]{3,2,1,0:T(8,128)S(1)}, f32[2,8,16,192]{3,2,1,0:T(8,128)}, u32[]{:S(2)}) copy-start(f32[2,8,16,192]{3,2,1,0:T(8,128)} %refs_5_.3) | copy-start | bytes 589828
  2.0 36.1 %all-to-all-start = ((bf16[64,8,128]{2,1,0:T(8,128)(2,1)}), bf16[64,8,128]{2,1,0:T(8,128)(2,1)S(1)}, u32[]{:S(2)}, u32[]{:S(2)}) async-start(bf16[64,8,128]{2,1,0:T(8,128)(2,1)} %broadcast_in_dim.3), calls=%async_computation | async-start | bytes 262144 | tf_op jit(solution)/shard_map/all_to_all | solution.py:18
  25.5 0.8 copy-start.6
  26.3 0.8 copy-start.7
  27.1 0.8 copy-start.8
  27.9 0.8 copy-start.9
  28.7 0.8 copy-start.10
  29.5 23.4 %collective-permute-start = (bf16[1,320,256]{2,1,0:T(8,128)(2,1)S(1)}, bf16[1,320,256]{2,1,0:T(8,128)(2,1)S(1)}, u32[]{:S(2)}, u32[]{:S(2)}) collective-permute-start(bf16[1,320,256]{2,1,0:T(8,128)(2,1)S(1)} %get-tuple-element.36), channel_id=1, source_target_pairs={{0,8},{1,9},{2,10},{3,11},{4,12},{5,13},{6,14},{7,15},{8,0},{9,1},... | collective-permute-start | bytes 491528 | tf_op jit(solution)/shard_map/ppermute | solution.py:27
  38.9 13.8 %all-to-all-start.1 = ((bf16[16,8,256]{2,1,0:T(8,128)(2,1)}), bf16[16,8,256]{2,1,0:T(8,128)(2,1)S(1)}, u32[]{:S(2)}, u32[]{:S(2)}) async-start(bf16[16,8,256]{2,1,0:T(8,128)(2,1)} %get-tuple-element.29), calls=%async_computation.1 | async-start | bytes 131072 | tf_op jit(solution)/shard_map/all_to_all | solution.py:18
  47.7 30.3 %copy-start.21 = (f32[2,32]{1,0:T(2,128)S(1)}, f32[2,32]{1,0:T(2,128)}, u32[]{:S(2)}) copy-start(f32[2,32]{1,0:T(2,128)} %param.18) | copy-start | bytes 772
  52.9 35.5 %copy-start.20 = (f32[2,8,16]{2,1,0:T(8,128)S(1)}, f32[2,8,16]{2,1,0:T(8,128)}, u32[]{:S(2)}) copy-start(f32[2,8,16]{2,1,0:T(8,128)} %param.23) | copy-start | bytes 3076
  52.9 21.7 %collective-permute-start.1 = (bf16[2,320,256]{2,1,0:T(8,128)(2,1)S(1)}, bf16[2,320,256]{2,1,0:T(8,128)(2,1)S(1)}, u32[]{:S(2)}, u32[]{:S(2)}) collective-permute-start(bf16[2,320,256]{2,1,0:T(8,128)(2,1)S(1)} %pad_maximum_fusion.2), channel_id=1, source_target_pairs={{0,4},{1,5},{2,6},{3,7},{4,0},{5,1},{6,2},{7,3},{8,12},{9,13},{10,... | collective-permute-start | bytes 983048 | tf_op jit(solution)/shard_map/ppermute | solution.py:27
  74.6 25.7 %copy-start.11 = (bf16[8,96]{1,0:T(8,128)(2,1)}, bf16[8,96]{1,0:T(8,128)(2,1)S(1)}, u32[]{:S(2)}) copy-start(bf16[8,96]{1,0:T(8,128)(2,1)S(1)} %get-tuple-element.47.vo_ref.refs_1_) | copy-start | bytes 4612
  74.7 25.7 %collective-permute-start.2 = (bf16[4,320,256]{2,1,0:T(8,128)(2,1)S(1)}, bf16[4,320,256]{2,1,0:T(8,128)(2,1)S(1)}, u32[]{:S(2)}, u32[]{:S(2)}) collective-permute-start(bf16[4,320,256]{2,1,0:T(8,128)(2,1)S(1)} %pad_maximum_fusion.1), channel_id=1, source_target_pairs={{0,2},{1,3},{2,0},{3,1},{4,6},{5,7},{6,4},{7,5},{8,10},{9,11},{10,... | collective-permute-start | bytes 1966088 | tf_op jit(solution)/shard_map/ppermute | solution.py:27
  78.0 21.9 %all-to-all-start.3 = ((bf16[64,8,128]{2,1,0:T(8,128)(2,1)}), bf16[64,8,128]{2,1,0:T(8,128)(2,1)S(1)}, u32[]{:S(2)}, u32[]{:S(2)}) async-start(bf16[64,8,128]{2,1,0:T(8,128)(2,1)} %get-tuple-element.32), calls=%async_computation.3 | async-start | bytes 262144 | tf_op jit(solution)/shard_map/all_to_all | solution.py:18
  100.4 19.4 %copy-start.15 = (bf16[8,64]{1,0:T(8,128)(2,1)S(1)}, bf16[8,64]{1,0:T(8,128)(2,1)}, u32[]{:S(2)}) copy-start(bf16[8,64]{1,0:T(8,128)(2,1)} %x_ref.1) | copy-start | bytes 3076
  100.5 19.2 %collective-permute-start.3 = (bf16[8,320,256]{2,1,0:T(8,128)(2,1)S(1)}, bf16[8,320,256]{2,1,0:T(8,128)(2,1)S(1)}, u32[]{:S(2)}, u32[]{:S(2)}) collective-permute-start(bf16[8,320,256]{2,1,0:T(8,128)(2,1)S(1)} %pad_maximum_fusion.held_ref), channel_id=1, source_target_pairs={{0,1},{1,0},{2,3},{3,2},{4,5},{5,4},{6,7},{7,6},{8,9},{9,8},{10,11... | collective-permute-start | bytes 3932168 | tf_op jit(solution)/shard_map/ppermute | solution.py:27
  119.8 5.8 %copy-start.17 = (f32[2,4096]{1,0:T(2,128)S(1)}, f32[2,4096]{1,0:T(2,128)}, u32[]{:S(2)}) copy-start(f32[2,4096]{1,0:T(2,128)} %param.20) | copy-start | bytes 98308
  121.0 17.4 %all-to-all-start.5 = ((bf16[64,8,128]{2,1,0:T(8,128)(2,1)}), bf16[64,8,128]{2,1,0:T(8,128)(2,1)S(1)}, u32[]{:S(2)}, u32[]{:S(2)}) async-start(bf16[64,8,128]{2,1,0:T(8,128)(2,1)} %shard_map.152), calls=%async_computation.5 | async-start | bytes 262144 | tf_op jit(solution)/shard_map/all_to_all | solution.py:18
  140.5 23.9 %copy-start.13 = (bf16[8,96]{1,0:T(8,128)(2,1)}, bf16[8,96]{1,0:T(8,128)(2,1)S(1)}, u32[]{:S(2)}) copy-start(bf16[8,96]{1,0:T(8,128)(2,1)S(1)} %get-tuple-element.43.vo_ref.refs_1_) | copy-start | bytes 4612
  140.5 17.4 %all-to-all-start.6 = ((bf16[64,8,128]{2,1,0:T(8,128)(2,1)}), bf16[64,8,128]{2,1,0:T(8,128)(2,1)S(1)}, u32[]{:S(2)}, u32[]{:S(2)}) async-start(bf16[64,8,128]{2,1,0:T(8,128)(2,1)} %get-tuple-element.39), calls=%async_computation.6 | async-start | bytes 262144 | tf_op jit(solution)/shard_map/all_to_all | solution.py:18
  157.9 6.5 %copy-start.3 = (bf16[64,8,128]{2,1,0:T(8,128)(2,1)}, bf16[64,8,128]{2,1,0:T(8,128)(2,1)S(1)}, u32[]{:S(2)}) copy-start(bf16[64,8,128]{2,1,0:T(8,128)(2,1)S(1)} %all-to-all-done.6.pieces_ref.refs_0_) | copy-start | bytes 393220
  159.0 18.0 %all-to-all-start.7 = ((bf16[64,8,128]{2,1,0:T(8,128)(2,1)}), bf16[64,8,128]{2,1,0:T(8,128)(2,1)}, u32[]{:S(2)}, u32[]{:S(2)}) async-start(bf16[64,8,128]{2,1,0:T(8,128)(2,1)} %shard_map.154), calls=%async_computation.7 | async-start | bytes 262144 | tf_op jit(solution)/shard_map/all_to_all | solution.py:18
  165.1 20.1 %copy-start = (f32[2,8,3,16,192]{4,3,2,1,0:T(8,128)S(1)}, f32[2,8,3,16,192]{4,3,2,1,0:T(8,128)}, u32[]{:S(2)}) copy-start(f32[2,8,3,16,192]{4,3,2,1,0:T(8,128)} %refs_4_.3) | copy-start | bytes 1769476
  176.9 0.7 copy-start.16
  179.7 9.3 %copy-start.18 = (f32[1,8,16]{2,1,0:T(8,128)S(1)}, f32[1,8,16]{2,1,0:T(8,128)}, u32[]{:S(2)}) copy-start(f32[1,8,16]{2,1,0:T(8,128)} %get-tuple-element.60) | copy-start | bytes 1540
  179.7 9.3 %copy-start.19 = (f32[1,8,16]{2,1,0:T(8,128)S(1)}, f32[1,8,16]{2,1,0:T(8,128)}, u32[]{:S(2)}) copy-start(f32[1,8,16]{2,1,0:T(8,128)} %get-tuple-element.63) | copy-start | bytes 1540
  179.7 9.9 %copy-start.4 = (bf16[64,8,128]{2,1,0:T(8,128)(2,1)S(1)}, bf16[64,8,128]{2,1,0:T(8,128)(2,1)}, u32[]{:S(2)}) copy-start(bf16[64,8,128]{2,1,0:T(8,128)(2,1)} %copy-done.3) | copy-start | bytes 393220
  179.7 9.9 %copy-start.14 = (bf16[8,96]{1,0:T(8,128)(2,1)S(1)}, bf16[8,96]{1,0:T(8,128)(2,1)}, u32[]{:S(2)}) copy-start(bf16[8,96]{1,0:T(8,128)(2,1)} %copy-done.13) | copy-start | bytes 4612
  179.7 17.4 %all-to-all-start.8 = ((bf16[64,8,128]{2,1,0:T(8,128)(2,1)}), bf16[64,8,128]{2,1,0:T(8,128)(2,1)S(1)}, u32[]{:S(2)}, u32[]{:S(2)}) async-start(bf16[64,8,128]{2,1,0:T(8,128)(2,1)} %copy-done.5), calls=%async_computation.8 | async-start | bytes 262144 | tf_op jit(solution)/shard_map/all_to_all | solution.py:18
  185.2 1.0 copy-start.2
  186.2 0.7 copy-start.12
  (1 other events, 0.7 us)

commit v4 on v3

--- a/solution.py
+++ b/solution.py
@@ -22,57 +22,35 @@
     return lax.optimization_barrier((x, earlier))[0]
 
 
-def step_of(held, bit):
+def to_chip(x, away):
     size = lax.axis_size("dp")
-    return lax.ppermute(held, "dp", [(i, i ^ bit) for i in range(size)])
-
-
-def merged(held, got):
-    return lax.optimization_barrier(jnp.concatenate([held, got]))
-
-
-def chain_order(size):
-    held, bit = [0], size // 2
-    while bit > 1:
-        held = held + [h ^ bit for h in held]
-        bit //= 2
-    return held
+    return lax.ppermute(x, "dp", [(i, (i + 2 * away) % size) for i in range(size)])
+
+
+def to_other_core(x):
+    size = lax.axis_size("dp")
+    return lax.ppermute(x, "dp", [(i, i ^ 1) for i in range(size)])
 
 
 def row_dot(x, turned):
     return lax.dot_general(x, turned, (((1,), (1,)), ((), ())), preferred_element_type=F32)
 
 
-class Weights:
-    def __init__(self, low, high, order, whole, held_ref, got_ref, buffer_ref, sems):
-        self.order, self.whole, self.buffer = order, whole, buffer_ref
-        self.copies = [
-            pltpu.make_async_copy(ref.at[:, low:high, :], buffer_ref.at[half], sems.at[half])
-            for half, ref in enumerate((held_ref, got_ref))
-        ]
-        for copy in self.copies:
-            copy.start()
-
-    def dot(self, x_ref):
-        me = lax.axis_index("dp")
-        base = me if self.whole else me & 1
-        rows = self.buffer.shape[3]
-        total = jnp.zeros((x_ref.shape[-2], self.buffer.shape[2]), F32)
-        for half, copy in enumerate(self.copies):
-            copy.wait()
-            for slot, other in enumerate(self.order):
-                at = base ^ (other ^ half)
-                if len(x_ref.shape) == 3:
-                    total = total + row_dot(x_ref[at], self.buffer[half, slot])
-                else:
-                    at = pl.multiple_of(at * rows, rows)
-                    total = total + row_dot(x_ref[:, pl.ds(at, rows)], self.buffer[half, slot])
-        return total
-
-
-def weight_space(held, columns):
-    shape = (2, held.shape[0], columns, held.shape[2])
-    return [pltpu.VMEM(shape, held.dtype), pltpu.SemaphoreType.DMA((2,))]
+def blocks_dot(x_ref, halves, places, low=0, high=None):
+    me = lax.axis_index("dp")
+    owners = 2 * len(places)
+    rows = halves[0].shape[2]
+    total = None
+    for half, ref in enumerate(halves):
+        for slot, away in enumerate(places):
+            at = lax.rem(me + (2 * away + owners), owners) ^ half
+            if len(x_ref.shape) == 3:
+                x = x_ref[at]
+            else:
+                x = x_ref[:, pl.ds(pl.multiple_of(at * rows, rows), rows)]
+            product = row_dot(x, ref[slot, low:high, :])
+            total = product if total is None else total + product
+    return total
 
 
 def pair_up(pieces_ref, width, at):
@@ -112,20 +90,30 @@
 
 
 def pack_kernel(*refs):
-    *project_refs, output_ref, own_ref, chain_ref = refs
+    count = (len(refs) - 3) // 2
+    given, (own_ref, ring_ref), found, sems = refs[:count], refs[count : count + 2], refs[count + 2 : -1], refs[-1]
+    fetches = [pltpu.make_async_copy(g, f, sems.at[k]) for k, (g, f) in enumerate(zip(given, found))]
+    for fetch in fetches:
+        fetch.start()
+    for fetch in fetches:
+        fetch.wait()
+    *projections, output = found
     at = 0
-    for ref in project_refs:
+    for ref in projections:
         size = ref.shape[1]
         own_ref[at : at + size, :] = ref[0]
-        chain_ref[0, at : at + size, :] = ref[1]
+        ring_ref[at : at + size, :] = ref[1]
         at += size
-    blocks, size, rows = output_ref.shape
+    blocks, size, rows = output.shape
     for block in range(blocks):
-        chain_ref[0, at : at + size, :rows] = output_ref[block]
-        chain_ref[0, at : at + size, rows:] = jnp.zeros(
-            (size, chain_ref.shape[2] - rows), chain_ref.dtype
-        )
+        ring_ref[at : at + size, :rows] = output[block]
+        ring_ref[at : at + size, rows:] = jnp.zeros((size, ring_ref.shape[1] - rows), ring_ref.dtype)
         at += size
+
+
+def stack_kernel(*refs):
+    for at, ref in enumerate(refs[:-1]):
+        refs[-1][at] = ref[...]
 
 
 def whole_kernel(pieces_ref, x_ref, cut_ref):
@@ -151,8 +139,7 @@
     vo_ref[...] = out[:, cut:].astype(vo_ref.dtype)
 
 
-def norm_kernel(cut, fetch, pieces_ref, gain_ref, held_ref, got_ref, x_ref, qk_ref, vo_ref, *space):
-    weights = Weights(*fetch, held_ref, got_ref, *space)
+def norm_kernel(cut, high, places, pieces_ref, gain_ref, held_ref, got_ref, x_ref, qk_ref, vo_ref):
     count, width = pieces_ref.shape[0], x_ref.shape[1] // pieces_ref.shape[0]
     pairs = [pair_up(pieces_ref, width, at) for at in range(count // 2)]
     features = x_ref.shape[1]
@@ -163,7 +150,7 @@
     for at, p in enumerate(pairs):
         cols = slice(2 * width * at, 2 * width * (at + 1))
         x_ref[:, cols] = (p * scale * gain_ref[:, cols]).astype(x_ref.dtype)
-    out = weights.dot(x_ref)
+    out = blocks_dot(x_ref, (held_ref, got_ref), places, 0, high)
     spread(qk_ref, out[:, :cut])
     vo_ref[...] = out[:, cut:].astype(vo_ref.dtype)
 
@@ -202,15 +189,14 @@
     spread(out_ref, jnp.concatenate(parts, axis=1))
 
 
-def branch_kernel(width, fetch, pieces_ref, x_ref, held_ref, got_ref, out_ref, wide_ref, *space):
-    weights = Weights(*fetch, held_ref, got_ref, *space)
+def branch_kernel(width, low, high, places, pieces_ref, x_ref, held_ref, got_ref, out_ref, wide_ref):
     blocks, seqs, rows = wide_ref.shape
     count = pieces_ref.shape[0] // blocks
     for at in range(blocks):
         found = [pieces_ref[count * at + k][:, :width].astype(F32) for k in range(count)]
         found.append(jnp.zeros((seqs, rows - count * width), F32))
         wide_ref[at] = jnp.concatenate(found, axis=1).astype(wide_ref.dtype)
-    branch = weights.dot(wide_ref)
+    branch = blocks_dot(wide_ref, (held_ref, got_ref), places, low, high)
     spread(out_ref, residual_scale * x_ref[...].astype(F32) + branch)
 
 
@@ -292,7 +278,8 @@
     rows, cols = query_weight.shape[1:]
     peers = lax.axis_size("tp")
     owners = lax.axis_size("dp")
-    order = chain_order(owners)
+    places = (0, -1, 1, -2, 2, -3, 3, -4)
+    assert owners == 2 * len(places)
     me = lax.axis_index("tp")
     bf16 = stream.dtype
     copies = jax.ShapeDtypeStruct((peers, seqs, LANES), bf16)
@@ -302,15 +289,16 @@
     turned = [jnp.swapaxes(w, 1, 2) for w in (query_weight, key_weight, value_weight, outgate_weight)]
     out_turned = jnp.swapaxes(output_weight, 1, 2)
     held_in = pl.BlockSpec(memory_space=pltpu.MemorySpace.HBM)
-    here = pl.BlockSpec(memory_space=pltpu.MemorySpace.VMEM)
-    own, chain = call(
+    given = (*turned, out_turned)
+    own, ring = call(
         pack_kernel,
         (
             jax.ShapeDtypeStruct((4 * cols, rows), bf16),
-            jax.ShapeDtypeStruct((1, 4 * cols + 2 * feats, rows), bf16),
+            jax.ShapeDtypeStruct((4 * cols + 2 * feats, rows), bf16),
         ),
-        *turned,
-        out_turned,
+        *given,
+        specs=[held_in] * len(given),
+        scratch=[*[pltpu.VMEM(w.shape, bf16) for w in given], pltpu.SemaphoreType.DMA((len(given),))],
     )
 
     def by_piece(x):
@@ -323,36 +311,36 @@
     whole_x = jax.ShapeDtypeStruct((seqs, peers * feats), bf16)
     tile = jnp.pad(stream, ((0, 0), (0, LANES - feats)))
     pieces = exchange(jnp.broadcast_to(tile, copies.shape), "tp")
-    got = step_of(chain, 8)
+    right, left = [to_chip(ring, 1)], [to_chip(ring, -1)]
     x_local = stream
     x_full, cut = call(
         whole_kernel, (whole_x, jax.ShapeDtypeStruct((owners, seqs, rows), bf16)), pieces
     )
     everyone = exchange(cut, "dp")
+    right.append(to_chip(right[-1], 1))
+    left.append(to_chip(left[-1], -1))
     partial = call(
         partial_kernel, jax.ShapeDtypeStruct((owners, seqs, 4 * cols), bf16), everyone, own
     )
     partial = after(partial, (states, normalizers))
     parts = exchange(partial, "dp")
-    chain = merged(after(chain, (partial,)), got)
-    got = step_of(chain, 4)
+    right.append(to_chip(right[-1], 1))
+    left.append(to_chip(left[-1], -1))
     saved, new_stabs = ([], [])
     for block_no in range(gate_bias.shape[0]):
         if block_no == 0:
             qk, vo = call(functools.partial(sum_kernel, 2 * cols), (copies, pair), parts)
-            chain = merged(after(chain, (qk,)), got)
-            got = step_of(chain, 2)
+            right.append(to_chip(right[-1], 1))
         else:
             x_full, qk, vo = call(
-                functools.partial(norm_kernel, 2 * cols, (0, 4 * cols, order, True)),
+                functools.partial(norm_kernel, 2 * cols, 4 * cols, places),
                 (whole_x, copies, pair),
                 pieces,
                 norm_gain[:1],
-                chain,
-                got,
-                specs=[here, here, held_in, held_in],
-                scratch=weight_space(chain, 4 * cols),
+                *halves,
             )
+            halves = after(halves, qk)
+            halves = [h[:, 4 * cols + feats :] for h in halves]
             x_local = lax.dynamic_slice_in_dim(x_full, me * feats, feats, 1)
             tied = after(saved[0], (qk,))
             made = update(0, tied, matrix_state, normalizer_state, ())
@@ -378,20 +366,25 @@
             normalizers[block_no],
         )
         if block_no == 0:
-            chain = merged(after(chain, (hidden,)), got)
-            got = step_of(chain, 1)
+            blocks = [ring]
+            for place in range(4):
+                blocks += [right[place], *left[place : place + 1]]
+            held = call(
+                stack_kernel,
+                jax.ShapeDtypeStruct((len(blocks), *ring.shape), bf16),
+                *after(blocks, hidden),
+            )
+            halves = (held, to_other_core(held))
         saved.append((pieces, vo, retain, admit))
         pieces = exchange(hidden, "tp")
-        low = 4 * cols + block_no * feats
+        low = 4 * cols * (1 - block_no)
         summed = call(
-            functools.partial(branch_kernel, cols, (low, low + feats, order, True)),
+            functools.partial(branch_kernel, cols, low, low + feats, places),
             copies,
             pieces,
             x_local,
-            chain,
-            got,
-            specs=[here, here, held_in, held_in],
-            scratch=[pltpu.VMEM((owners, seqs, rows), bf16), *weight_space(chain, feats)],
+            *halves,
+            scratch=[pltpu.VMEM((owners, seqs, rows), bf16)],
         )
         new_stabs.append(stab_new)
         pieces = exchange(summed, "tp")

time: 199 us -> 198 us (level)
  the two profiles are of different devices: /device:TPU:2 before, /device:TPU:16 now
where the time goes in v4:
time: 198 us; the launch traced here: 197 us
  starting transfers between devices  93.3 us (47%)
  waiting for transfers between devices  46.8 us (24%)
  blocking collectives  25.1 us (13%)
  local copies, waits for them, and re-layouts  13.3 us (7%)
  Pallas kernels  13.1 us (7%)
  matrix products  2.24 us (1%)
  other arithmetic  1.99 us (1%)
    all_to_all x8, starting transfers between devices, exchange(): return lax.all_to_all(pieces, axis, split_axis=0, concat_axis=0, tiled=True)  67.6 us
    all_to_all x8, waiting for transfers between devices, exchange(): return lax.all_to_all(pieces, axis, split_axis=0, concat_axis=0, tiled=True)  45.7 us
    all_to_all x1, blocking collectives, exchange(): return lax.all_to_all(pieces, axis, split_axis=0, concat_axis=0, tiled=True)  25.1 us
    ppermute x7, starting transfers between devices, to_chip(): lax.ppermute(x, 'dp', [(i, (i + 2 * away) % size) for i in range(size)])  23.7 us
    pallas_call x13, Pallas kernels, call(): pl.pallas_call(kernel, out_shape=out_shape, scratch_shapes=list(scratch),...  13.1 us
    unnamed x48, local copies, waits for them, and re-layouts  6.35 us
  transfers between devices with their start and end apart: 16, of which 8 were waited for; matrix products, arithmetic and copies ran while one was open for 5% of the time, Pallas kernels for 4%

profile of v4, /device:TPU:16, one launch (start us, length us, event | category | flops | bytes accessed | tf_op | source)
XLA Modules:
  0.0 196.8 jit_solution(5777077329633556259)
XLA Ops:
  2.0 23.3 %all-to-all-start = ((bf16[64,8,128]{2,1,0:T(8,128)(2,1)}), bf16[64,8,128]{2,1,0:T(8,128)(2,1)S(1)}, u32[]{:S(2)}, u32[]{:S(2)}) async-start(bf16[64,8,128]{2,1,0:T(8,128)(2,1)} %broadcast_in_dim.3), calls=%async_computation | async-start | bytes 262144 | tf_op jit(solution)/shard_map/all_to_all | solution.py:18
  29.8 4.8 %collective-permute-start.1 = (bf16[320,256]{1,0:T(8,128)(2,1)S(1)}, bf16[320,256]{1,0:T(8,128)(2,1)S(1)}, u32[]{:S(2)}, u32[]{:S(2)}) collective-permute-start(bf16[320,256]{1,0:T(8,128)(2,1)S(1)} %get-tuple-element.43.refs_0_), channel_id=1, source_target_pairs={{0,14},{1,15},{2,0},{3,1},{4,2},{5,3},{6,4},{7,5},{8,6},{9,7},{10,... | collective-permute-start | bytes 491528 | tf_op jit(solution)/shard_map/ppermute | solution.py:27
  34.6 1.9 collective-permute-start
  36.5 1.2 fusion.10
  38.4 6.4 %all-to-all-start.1 = ((bf16[16,8,256]{2,1,0:T(8,128)(2,1)}), bf16[16,8,256]{2,1,0:T(8,128)(2,1)S(1)}, u32[]{:S(2)}, u32[]{:S(2)}) async-start(bf16[16,8,256]{2,1,0:T(8,128)(2,1)} %get-tuple-element.36), calls=%async_computation.1 | async-start | bytes 131072 | tf_op jit(solution)/shard_map/all_to_all | solution.py:18
  46.4 3.8 %collective-permute-start.2 = (bf16[320,256]{1,0:T(8,128)(2,1)S(1)}, bf16[320,256]{1,0:T(8,128)(2,1)S(1)}, u32[]{:S(2)}, u32[]{:S(2)}) collective-permute-start(bf16[320,256]{1,0:T(8,128)(2,1)S(1)} %collective-permute-done.refs_1_), channel_id=1, source_target_pairs={{0,2},{1,3},{2,4},{3,5},{4,6},{5,7},{6,8},{7,9},{8,10},{9,11},{10,... | collective-permute-start | bytes 491528 | tf_op jit(solution)/shard_map/ppermute | solution.py:27
  50.2 2.5 %all-to-all-done.1.x_ref = bf16[16,8,256]{2,1,0:T(8,128)(2,1)S(1)} async-done(((bf16[16,8,256]{2,1,0:T(8,128)(2,1)}), bf16[16,8,256]{2,1,0:T(8,128)(2,1)S(1)}, u32[]{:S(2)}, u32[]{:S(2)}) %all-to-all-start.1) | async-done | bytes 65568 | tf_op jit(solution)/shard_map/all_to_all | solution.py:18
  53.5 3.5 %all-to-all-start.2 = ((bf16[16,8,192]{2,1,0:T(8,128)(2,1)}), bf16[16,8,192]{2,1,0:T(8,128)(2,1)S(1)}, u32[]{:S(2)}, u32[]{:S(2)}) async-start(bf16[16,8,192]{2,1,0:T(8,128)(2,1)} %shard_map.149), calls=%async_computation.2 | async-start | bytes 131072 | tf_op jit(solution)/shard_map/all_to_all | solution.py:18
  57.1 5.0 %collective-permute-start.3 = (bf16[320,256]{1,0:T(8,128)(2,1)S(1)}, bf16[320,256]{1,0:T(8,128)(2,1)S(1)}, u32[]{:S(2)}, u32[]{:S(2)}) collective-permute-start(bf16[320,256]{1,0:T(8,128)(2,1)S(1)} %collective-permute-done.1.refs_2_), channel_id=1, source_target_pairs={{0,14},{1,15},{2,0},{3,1},{4,2},{5,3},{6,4},{7,5},{8,6},{9,7},{10,... | collective-permute-start | bytes 491528 | tf_op jit(solution)/shard_map/ppermute | solution.py:27
  62.1 1.9 collective-permute-start.4
  65.5 12.3 %all-to-all-start.3 = ((bf16[64,8,128]{2,1,0:T(8,128)(2,1)}), bf16[64,8,128]{2,1,0:T(8,128)(2,1)S(1)}, u32[]{:S(2)}, u32[]{:S(2)}) async-start(bf16[64,8,128]{2,1,0:T(8,128)(2,1)} %get-tuple-element.39), calls=%async_computation.3 | async-start | bytes 262144 | tf_op jit(solution)/shard_map/all_to_all | solution.py:18
  77.8 1.1 convolution_add_fusion.1
  78.9 4.4 %collective-permute-start.5 = (bf16[320,256]{1,0:T(8,128)(2,1)S(1)}, bf16[320,256]{1,0:T(8,128)(2,1)S(1)}, u32[]{:S(2)}, u32[]{:S(2)}) collective-permute-start(bf16[320,256]{1,0:T(8,128)(2,1)S(1)} %collective-permute-done.3.refs_4_), channel_id=1, source_target_pairs={{0,14},{1,15},{2,0},{3,1},{4,2},{5,3},{6,4},{7,5},{8,6},{9,7},{10,... | collective-permute-start | bytes 491528 | tf_op jit(solution)/shard_map/ppermute | solution.py:27
  83.3 1.9 collective-permute-start.6
  85.9 4.2 %all-to-all-done.3.pieces_ref.refs_0_ = bf16[64,8,128]{2,1,0:T(8,128)(2,1)S(1)} async-done(((bf16[64,8,128]{2,1,0:T(8,128)(2,1)}), bf16[64,8,128]{2,1,0:T(8,128)(2,1)S(1)}, u32[]{:S(2)}, u32[]{:S(2)}) %all-to-all-start.3) | async-done | bytes 131104 | tf_op jit(solution)/shard_map/all_to_all | solution.py:18
  90.6 1.1 collective-permute-done.6.refs_7_
  91.8 1.9 collective-permute-start.7
  93.7 25.1 %all_to_all.45.pieces_ref = bf16[64,8,128]{2,1,0:T(8,128)(2,1)S(1)} all-to-all(bf16[64,8,128]{2,1,0:T(8,128)(2,1)S(1)} %shard_map.151), channel_id=1, replica_groups=mesh['tp'=64,'dp'=16] {'tp'}, dimensions={0} | all-to-all | bytes 262144 | tf_op jit(solution)/shard_map/all_to_all | solution.py:18
  118.8 1.0 shard_map.153
  119.8 5.2 %all-to-all-start.5 = ((bf16[64,8,128]{2,1,0:T(8,128)(2,1)}), bf16[64,8,128]{2,1,0:T(8,128)(2,1)S(1)}, u32[]{:S(2)}, u32[]{:S(2)}) async-start(bf16[64,8,128]{2,1,0:T(8,128)(2,1)} %shard_map.153), calls=%async_computation.5 | async-start | bytes 262144 | tf_op jit(solution)/shard_map/all_to_all | solution.py:18
  125.7 11.4 %all-to-all-done.5.pieces_ref = bf16[64,8,128]{2,1,0:T(8,128)(2,1)S(1)} async-done(((bf16[64,8,128]{2,1,0:T(8,128)(2,1)}), bf16[64,8,128]{2,1,0:T(8,128)(2,1)S(1)}, u32[]{:S(2)}, u32[]{:S(2)}) %all-to-all-start.5) | async-done | bytes 131104 | tf_op jit(solution)/shard_map/all_to_all | solution.py:18
  137.0 1.5 shard_map.154
  138.5 5.4 %all-to-all-start.6 = ((bf16[64,8,128]{2,1,0:T(8,128)(2,1)}), bf16[64,8,128]{2,1,0:T(8,128)(2,1)S(1)}, u32[]{:S(2)}, u32[]{:S(2)}) async-start(bf16[64,8,128]{2,1,0:T(8,128)(2,1)} %get-tuple-element.51), calls=%async_computation.6 | async-start | bytes 262144 | tf_op jit(solution)/shard_map/all_to_all | solution.py:18
  143.9 1.1 convolution_add_fusion
  145.7 10.2 %all-to-all-done.6.pieces_ref.refs_0_ = bf16[64,8,128]{2,1,0:T(8,128)(2,1)S(1)} async-done(((bf16[64,8,128]{2,1,0:T(8,128)(2,1)}), bf16[64,8,128]{2,1,0:T(8,128)(2,1)S(1)}, u32[]{:S(2)}, u32[]{:S(2)}) %all-to-all-start.6) | async-done | bytes 131104 | tf_op jit(solution)/shard_map/all_to_all | solution.py:18
  157.7 6.2 %all-to-all-start.7 = ((bf16[64,8,128]{2,1,0:T(8,128)(2,1)}), bf16[64,8,128]{2,1,0:T(8,128)(2,1)}, u32[]{:S(2)}, u32[]{:S(2)}) async-start(bf16[64,8,128]{2,1,0:T(8,128)(2,1)} %copy-done.6), calls=%async_computation.7 | async-start | bytes 262144 | tf_op jit(solution)/shard_map/all_to_all | solution.py:18
  165.5 10.3 %all-to-all-done.7.pieces_ref = bf16[64,8,128]{2,1,0:T(8,128)(2,1)} async-done(((bf16[64,8,128]{2,1,0:T(8,128)(2,1)}), bf16[64,8,128]{2,1,0:T(8,128)(2,1)}, u32[]{:S(2)}, u32[]{:S(2)}) %all-to-all-start.7) | async-done | bytes 131104 | tf_op jit(solution)/shard_map/all_to_all | solution.py:18
  176.8 1.9 shard_map.156
  178.7 5.3 %all-to-all-start.8 = ((bf16[64,8,128]{2,1,0:T(8,128)(2,1)}), bf16[64,8,128]{2,1,0:T(8,128)(2,1)S(1)}, u32[]{:S(2)}, u32[]{:S(2)}) async-start(bf16[64,8,128]{2,1,0:T(8,128)(2,1)} %shard_map.156), calls=%async_computation.8 | async-start | bytes 262144 | tf_op jit(solution)/shard_map/all_to_all | solution.py:18
  184.7 2.2 %shard_map.158 = (f32[2,8,3,16,192]{4,3,2,1,0:T(8,128)}, f32[2,8,16,192]{3,2,1,0:T(8,128)}) custom-call(bf16[64,8,128]{2,1,0:T(8,128)(2,1)S(1)} %all-to-all-done.3.pieces_ref.refs_0_, bf16[8,96]{1,0:T(8,128)(2,1)S(1)} %copy-done.14, f32[8,16]{1,0:T(8,128)S(1)} %get-tuple-element.62.retain_ref.refs_2_, f32[8,16]{1,0:T(8,128)S(1)} %get-tuple-element.63.admit_ref.refs_3_, ...), custom_call_target="tpu_custom_call" | custom-call | flops 1000000 | bytes 920064 | tf_op jit(solution)/shard_map/pallas_call | solution.py:76
  187.5 2.2 %shard_map.159 = (f32[2,8,3,16,192]{4,3,2,1,0:T(8,128)}, f32[2,8,16,192]{3,2,1,0:T(8,128)}) custom-call(bf16[64,8,128]{2,1,0:T(8,128)(2,1)S(1)} %copy-done.4, bf16[8,96]{1,0:T(8,128)(2,1)S(1)} %copy-done.16, f32[8,16]{1,0:T(8,128)S(1)} %get-tuple-element.58.retain_ref.refs_2_, ...), custom_call_target="tpu_custom_call", output_to_operand_aliasing={{0}: (6, {}), {1}: (7, {})} | custom-call | flops 1000000 | bytes 1706496 | tf_op jit(solution)/shard_map/pallas_call | solution.py:76
  189.7 6.3 %all-to-all-done.8.pieces_ref = bf16[64,8,128]{2,1,0:T(8,128)(2,1)S(1)} async-done(((bf16[64,8,128]{2,1,0:T(8,128)(2,1)}), bf16[64,8,128]{2,1,0:T(8,128)(2,1)S(1)}, u32[]{:S(2)}, u32[]{:S(2)}) %all-to-all-start.8) | async-done | bytes 131104 | tf_op jit(solution)/shard_map/all_to_all | solution.py:18
  (85 shorter events, 19.3 us)
Async XLA Ops:
  0.6 44.2 %copy-start.1 = (f32[2,8,16,192]{3,2,1,0:T(8,128)S(1)}, f32[2,8,16,192]{3,2,1,0:T(8,128)}, u32[]{:S(2)}) copy-start(f32[2,8,16,192]{3,2,1,0:T(8,128)} %refs_5_.3) | copy-start | bytes 589828
  2.0 35.6 %all-to-all-start = ((bf16[64,8,128]{2,1,0:T(8,128)(2,1)}), bf16[64,8,128]{2,1,0:T(8,128)(2,1)S(1)}, u32[]{:S(2)}, u32[]{:S(2)}) async-start(bf16[64,8,128]{2,1,0:T(8,128)(2,1)} %broadcast_in_dim.3), calls=%async_computation | async-start | bytes 262144 | tf_op jit(solution)/shard_map/all_to_all | solution.py:18
  29.8 27.3 %collective-permute-start.1 = (bf16[320,256]{1,0:T(8,128)(2,1)S(1)}, bf16[320,256]{1,0:T(8,128)(2,1)S(1)}, u32[]{:S(2)}, u32[]{:S(2)}) collective-permute-start(bf16[320,256]{1,0:T(8,128)(2,1)S(1)} %get-tuple-element.43.refs_0_), channel_id=1, source_target_pairs={{0,14},{1,15},{2,0},{3,1},{4,2},{5,3},{6,4},{7,5},{8,6},{9,7},{10,... | collective-permute-start | bytes 491528 | tf_op jit(solution)/shard_map/ppermute | solution.py:27
  34.6 11.8 %collective-permute-start = (bf16[320,256]{1,0:T(8,128)(2,1)S(1)}, bf16[320,256]{1,0:T(8,128)(2,1)S(1)}, u32[]{:S(2)}, u32[]{:S(2)}) collective-permute-start(bf16[320,256]{1,0:T(8,128)(2,1)S(1)} %get-tuple-element.43.refs_0_), channel_id=1, source_target_pairs={{0,2},{1,3},{2,4},{3,5},{4,6},{5,7},{6,8},{7,9},{8,10},{9,11},{10,... | collective-permute-start | bytes 491528 | tf_op jit(solution)/shard_map/ppermute | solution.py:27
  38.4 14.3 %all-to-all-start.1 = ((bf16[16,8,256]{2,1,0:T(8,128)(2,1)}), bf16[16,8,256]{2,1,0:T(8,128)(2,1)S(1)}, u32[]{:S(2)}, u32[]{:S(2)}) async-start(bf16[16,8,256]{2,1,0:T(8,128)(2,1)} %get-tuple-element.36), calls=%async_computation.1 | async-start | bytes 131072 | tf_op jit(solution)/shard_map/all_to_all | solution.py:18
  45.6 11.4 %copy-start.23 = (f32[2,32]{1,0:T(2,128)S(1)}, f32[2,32]{1,0:T(2,128)}, u32[]{:S(2)}) copy-start(f32[2,32]{1,0:T(2,128)} %param.18) | copy-start | bytes 772
  45.8 39.4 %copy-start.21 = (f32[2,8,16]{2,1,0:T(8,128)S(1)}, f32[2,8,16]{2,1,0:T(8,128)}, u32[]{:S(2)}) copy-start(f32[2,8,16]{2,1,0:T(8,128)} %param.23) | copy-start | bytes 3076
  46.4 15.7 %collective-permute-start.2 = (bf16[320,256]{1,0:T(8,128)(2,1)S(1)}, bf16[320,256]{1,0:T(8,128)(2,1)S(1)}, u32[]{:S(2)}, u32[]{:S(2)}) collective-permute-start(bf16[320,256]{1,0:T(8,128)(2,1)S(1)} %collective-permute-done.refs_1_), channel_id=1, source_target_pairs={{0,2},{1,3},{2,4},{3,5},{4,6},{5,7},{6,8},{7,9},{8,10},{9,11},{10,... | collective-permute-start | bytes 491528 | tf_op jit(solution)/shard_map/ppermute | solution.py:27
  53.5 11.3 %all-to-all-start.2 = ((bf16[16,8,192]{2,1,0:T(8,128)(2,1)}), bf16[16,8,192]{2,1,0:T(8,128)(2,1)S(1)}, u32[]{:S(2)}, u32[]{:S(2)}) async-start(bf16[16,8,192]{2,1,0:T(8,128)(2,1)} %shard_map.149), calls=%async_computation.2 | async-start | bytes 131072 | tf_op jit(solution)/shard_map/all_to_all | solution.py:18
  57.1 21.8 %collective-permute-start.3 = (bf16[320,256]{1,0:T(8,128)(2,1)S(1)}, bf16[320,256]{1,0:T(8,128)(2,1)S(1)}, u32[]{:S(2)}, u32[]{:S(2)}) collective-permute-start(bf16[320,256]{1,0:T(8,128)(2,1)S(1)} %collective-permute-done.1.refs_2_), channel_id=1, source_target_pairs={{0,14},{1,15},{2,0},{3,1},{4,2},{5,3},{6,4},{7,5},{8,6},{9,7},{10,... | collective-permute-start | bytes 491528 | tf_op jit(solution)/shard_map/ppermute | solution.py:27
  62.1 21.2 %collective-permute-start.4 = (bf16[320,256]{1,0:T(8,128)(2,1)S(1)}, bf16[320,256]{1,0:T(8,128)(2,1)S(1)}, u32[]{:S(2)}, u32[]{:S(2)}) collective-permute-start(bf16[320,256]{1,0:T(8,128)(2,1)S(1)} %collective-permute-done.2.refs_3_), channel_id=1, source_target_pairs={{0,2},{1,3},{2,4},{3,5},{4,6},{5,7},{6,8},{7,9},{8,10},{9,11},{10,... | collective-permute-start | bytes 491528 | tf_op jit(solution)/shard_map/ppermute | solution.py:27
  65.5 25.1 %copy-start.13 = (bf16[8,96]{1,0:T(8,128)(2,1)}, bf16[8,96]{1,0:T(8,128)(2,1)S(1)}, u32[]{:S(2)}) copy-start(bf16[8,96]{1,0:T(8,128)(2,1)S(1)} %get-tuple-element.61.vo_ref.refs_1_) | copy-start | bytes 4612
  65.5 24.6 %all-to-all-start.3 = ((bf16[64,8,128]{2,1,0:T(8,128)(2,1)}), bf16[64,8,128]{2,1,0:T(8,128)(2,1)S(1)}, u32[]{:S(2)}, u32[]{:S(2)}) async-start(bf16[64,8,128]{2,1,0:T(8,128)(2,1)} %get-tuple-element.39), calls=%async_computation.3 | async-start | bytes 262144 | tf_op jit(solution)/shard_map/all_to_all | solution.py:18
  78.9 11.6 %collective-permute-start.5 = (bf16[320,256]{1,0:T(8,128)(2,1)S(1)}, bf16[320,256]{1,0:T(8,128)(2,1)S(1)}, u32[]{:S(2)}, u32[]{:S(2)}) collective-permute-start(bf16[320,256]{1,0:T(8,128)(2,1)S(1)} %collective-permute-done.3.refs_4_), channel_id=1, source_target_pairs={{0,14},{1,15},{2,0},{3,1},{4,2},{5,3},{6,4},{7,5},{8,6},{9,7},{10,... | collective-permute-start | bytes 491528 | tf_op jit(solution)/shard_map/ppermute | solution.py:27
  83.3 8.4 %collective-permute-start.6 = (bf16[320,256]{1,0:T(8,128)(2,1)S(1)}, bf16[320,256]{1,0:T(8,128)(2,1)S(1)}, u32[]{:S(2)}, u32[]{:S(2)}) collective-permute-start(bf16[320,256]{1,0:T(8,128)(2,1)S(1)} %collective-permute-done.4.refs_5_), channel_id=1, source_target_pairs={{0,2},{1,3},{2,4},{3,5},{4,6},{5,7},{6,8},{7,9},{8,10},{9,11},{10,... | collective-permute-start | bytes 491528 | tf_op jit(solution)/shard_map/ppermute | solution.py:27
  90.5 28.3 %copy-start.17 = (bf16[8,64]{1,0:T(8,128)(2,1)S(1)}, bf16[8,64]{1,0:T(8,128)(2,1)}, u32[]{:S(2)}) copy-start(bf16[8,64]{1,0:T(8,128)(2,1)} %x_ref.1) | copy-start | bytes 3076
  91.8 27.0 %collective-permute-start.7 = (bf16[8,320,256]{2,1,0:T(8,128)(2,1)S(1)}, bf16[8,320,256]{2,1,0:T(8,128)(2,1)S(1)}, u32[]{:S(2)}, u32[]{:S(2)}) collective-permute-start(bf16[8,320,256]{2,1,0:T(8,128)(2,1)S(1)} %shard_map.152.held_ref), channel_id=1, source_target_pairs={{0,1},{1,0},{2,3},{3,2},{4,5},{5,4},{6,7},{7,6},{8,9},{9,8},{10,11... | collective-permute-start | bytes 3932168 | tf_op jit(solution)/shard_map/ppermute | solution.py:32
  118.8 6.2 %copy-start.18 = (f32[2,4096]{1,0:T(2,128)S(1)}, f32[2,4096]{1,0:T(2,128)}, u32[]{:S(2)}) copy-start(f32[2,4096]{1,0:T(2,128)} %param.20) | copy-start | bytes 98308
  119.8 17.2 %all-to-all-start.5 = ((bf16[64,8,128]{2,1,0:T(8,128)(2,1)}), bf16[64,8,128]{2,1,0:T(8,128)(2,1)S(1)}, u32[]{:S(2)}, u32[]{:S(2)}) async-start(bf16[64,8,128]{2,1,0:T(8,128)(2,1)} %shard_map.153), calls=%async_computation.5 | async-start | bytes 262144 | tf_op jit(solution)/shard_map/all_to_all | solution.py:18
  137.0 8.0 %copy-start.22 = (f32[2,8,16]{2,1,0:T(8,128)S(1)}, f32[2,8,16]{2,1,0:T(8,128)}, u32[]{:S(2)}) copy-start(f32[2,8,16]{2,1,0:T(8,128)} %param.23) | copy-start | bytes 3076
  138.5 17.4 %copy-start.7 = (bf16[8,4096]{1,0:T(8,128)(2,1)}, bf16[8,4096]{1,0:T(8,128)(2,1)S(1)}, u32[]{:S(2)}) copy-start(bf16[8,4096]{1,0:T(8,128)(2,1)S(1)} %get-tuple-element.53) | copy-start | bytes 196612
  138.5 17.4 %copy-start.15 = (bf16[8,96]{1,0:T(8,128)(2,1)}, bf16[8,96]{1,0:T(8,128)(2,1)S(1)}, u32[]{:S(2)}) copy-start(bf16[8,96]{1,0:T(8,128)(2,1)S(1)} %get-tuple-element.57.vo_ref.refs_1_) | copy-start | bytes 4612
  138.5 17.4 %all-to-all-start.6 = ((bf16[64,8,128]{2,1,0:T(8,128)(2,1)}), bf16[64,8,128]{2,1,0:T(8,128)(2,1)S(1)}, u32[]{:S(2)}, u32[]{:S(2)}) async-start(bf16[64,8,128]{2,1,0:T(8,128)(2,1)} %get-tuple-element.51), calls=%async_computation.6 | async-start | bytes 262144 | tf_op jit(solution)/shard_map/all_to_all | solution.py:18
  157.6 27.0 %copy-start = (f32[2,8,3,16,192]{4,3,2,1,0:T(8,128)S(1)}, f32[2,8,3,16,192]{4,3,2,1,0:T(8,128)}, u32[]{:S(2)}) copy-start(f32[2,8,3,16,192]{4,3,2,1,0:T(8,128)} %refs_4_.3) | copy-start | bytes 1769476
  157.7 18.2 %all-to-all-start.7 = ((bf16[64,8,128]{2,1,0:T(8,128)(2,1)}), bf16[64,8,128]{2,1,0:T(8,128)(2,1)}, u32[]{:S(2)}, u32[]{:S(2)}) async-start(bf16[64,8,128]{2,1,0:T(8,128)(2,1)} %copy-done.6), calls=%async_computation.7 | async-start | bytes 262144 | tf_op jit(solution)/shard_map/all_to_all | solution.py:18
  164.6 20.1 %copy-start.2 = (f32[2,8,16,192]{3,2,1,0:T(8,128)S(1)}, f32[2,8,16,192]{3,2,1,0:T(8,128)}, u32[]{:S(2)}) copy-start(f32[2,8,16,192]{3,2,1,0:T(8,128)} %refs_5_.3) | copy-start | bytes 589828
  164.6 20.1 %copy-start.14 = (bf16[8,96]{1,0:T(8,128)(2,1)S(1)}, bf16[8,96]{1,0:T(8,128)(2,1)}, u32[]{:S(2)}) copy-start(bf16[8,96]{1,0:T(8,128)(2,1)} %copy-done.13) | copy-start | bytes 4612
  164.6 22.3 %copy-start.19 = (f32[1,8,16]{2,1,0:T(8,128)S(1)}, f32[1,8,16]{2,1,0:T(8,128)}, u32[]{:S(2)}) copy-start(f32[1,8,16]{2,1,0:T(8,128)} %get-tuple-element.74) | copy-start | bytes 1540
  164.6 22.3 %copy-start.20 = (f32[1,8,16]{2,1,0:T(8,128)S(1)}, f32[1,8,16]{2,1,0:T(8,128)}, u32[]{:S(2)}) copy-start(f32[1,8,16]{2,1,0:T(8,128)} %get-tuple-element.77) | copy-start | bytes 1540
  164.6 22.9 %copy-start.4 = (bf16[64,8,128]{2,1,0:T(8,128)(2,1)S(1)}, bf16[64,8,128]{2,1,0:T(8,128)(2,1)}, u32[]{:S(2)}) copy-start(bf16[64,8,128]{2,1,0:T(8,128)(2,1)} %copy-done.3) | copy-start | bytes 393220
  164.6 22.9 %copy-start.16 = (bf16[8,96]{1,0:T(8,128)(2,1)S(1)}, bf16[8,96]{1,0:T(8,128)(2,1)}, u32[]{:S(2)}) copy-start(bf16[8,96]{1,0:T(8,128)(2,1)} %copy-done.15) | copy-start | bytes 4612
  178.7 17.3 %all-to-all-start.8 = ((bf16[64,8,128]{2,1,0:T(8,128)(2,1)}), bf16[64,8,128]{2,1,0:T(8,128)(2,1)S(1)}, u32[]{:S(2)}, u32[]{:S(2)}) async-start(bf16[64,8,128]{2,1,0:T(8,128)(2,1)} %shard_map.156), calls=%async_computation.8 | async-start | bytes 262144 | tf_op jit(solution)/shard_map/all_to_all | solution.py:18
  (8 other events, 6.3 us)
